TPU v7x, 32 devices: a whole 2x2x4 slice. The times are simulated.
32 devices in a mesh: sp: 16 (over z, y, x), tp: 2 (over core).
Axes of the slice: x: 2, y: 2, z: 4, core: 2. Of those that a mesh axis runs over, the one named last changes fastest.
Arguments:
- stream: bfloat16 [4096, 2048], P('sp', 'tp'), may hold values from -6 to 6
- out_grad: bfloat16 [4096, 2048], P('sp', 'tp'), may hold values from -6 to 6
- gate_in: bfloat16 [4096, 1024], P('sp', 'tp'), may hold values from -6 to 6
- conv_gate: bfloat16 [4096, 1024], P('sp', 'tp'), may hold values from -6 to 6
- conv_value: bfloat16 [4096, 1024], P('sp', 'tp'), may hold values from -6 to 6
- taps: float32 [3, 1024], P(None, 'tp'), may hold values from -3.5 to 3.5
- w_out: bfloat16 [2048, 1024], P(None, 'tp'), may hold values from -0.1875 to 0.1875
- route_ids: int32 [4096, 2], P('sp'), may hold values from 0 to 15, all different within a row; in each aligned block of 256 rows (0 to 255, 256 to 511, ...) at most 64 rows name the same one
- route_weights: float32 [4096, 2], P('sp'), may hold values from 0.1 to 1
- w_gate: bfloat16 [16, 2048, 1024], P('sp', None, 'tp'), may hold values from -0.125 to 0.125
- w_up: bfloat16 [16, 2048, 1024], P('sp', None, 'tp'), may hold values from -0.125 to 0.125
- w_down: bfloat16 [16, 1024, 2048], P('sp', 'tp'), may hold values from -0.1875 to 0.1875
Outputs:
- stream_grad: bfloat16 [4096, 2048], P('sp', 'tp')
- gate_in_grad: bfloat16 [4096, 1024], P('sp', 'tp')
- conv_gate_grad: bfloat16 [4096, 1024], P('sp', 'tp')
- conv_value_grad: bfloat16 [4096, 1024], P('sp', 'tp')
- w_out_grad: float32 [2048, 1024], P('sp', 'tp')
- w_gate_grad: float32 [16, 2048, 1024], P('sp', None, 'tp')
- w_up_grad: float32 [16, 2048, 1024], P('sp', None, 'tp')
- w_down_grad: float32 [16, 1024, 2048], P('sp', 'tp')
Inputs may be any that keep to these rules, and one draw needn't show every extreme that they name: `route_ids`: the ids of one token differ. Within each aligned block of 256 tokens (the rows of one index of sp), no expert is named by more than 64 routes, and in every draw some expert is named by exactly 64 routes of some block.
All inputs are finite; a program needn't handle non-finite values.
Results may differ from a plain program's by a relative error of at most 0.009.
Values may be sent and summed in bfloat16 or wider, within the bound.
No kernel may reach another device: no remote copies, remote signals or barrier semaphores. Data moves between devices by JAX's collectives and lax.ppermute only.
A program may use at most 128 MiB of HBM per device.

v0:
```python
import jax
import jax.numpy as jnp
from jax import lax
from jax.sharding import PartitionSpec as P

BF = jnp.bfloat16
F32 = jnp.float32


def passed_along(shard, axis, by):
    count = lax.axis_size(axis)
    pairs = [(i, i + by) for i in range(count) if 0 <= i + by < count]
    return lax.ppermute(shard, axis, pairs)


def swapped(shard):
    return lax.ppermute(shard, "tp", [(0, 1), (1, 0)])


def exchanged(blocks, groups=None):
    return lax.all_to_all(
        blocks, "sp", split_axis=0, concat_axis=0, tiled=True, axis_index_groups=groups
    )


def in_order(mine, other, first, axis):
    return jnp.where(
        first,
        jnp.concatenate([mine, other], axis=axis),
        jnp.concatenate([other, mine], axis=axis),
    )


def mm(left, right, dims):
    return lax.dot_general(left, right, (dims, ((), ())), preferred_element_type=F32)


def shards(
    stream,
    out_grad,
    gate_in,
    conv_gate,
    conv_value,
    taps,
    w_out,
    route_ids,
    route_weights,
    w_gate,
    w_up,
    w_down,
):
    tok_rows, half_width = stream.shape
    width = 2 * half_width
    sp_count = lax.axis_size("sp")
    experts = w_gate.shape[0] * sp_count
    capacity = 4 * tok_rows // experts
    part = capacity // 2
    slots = experts * part
    tp = lax.axis_index("tp")
    first = tp == 0

    half = sp_count // 2
    half_experts = experts // 2
    upper = lax.axis_index("sp") >= half

    def traded(shard):
        return lax.ppermute(shard, "sp", [(i, i ^ half) for i in range(sp_count)])

    facts = jnp.concatenate([route_ids.T.astype(F32), route_weights.T], axis=0)
    facts = jnp.concatenate([facts, traded(facts)], axis=1)
    stream_there = traded(stream)
    out_there = traded(out_grad)
    stream_full = in_order(stream, swapped(stream), first, 1)
    out_full = in_order(out_grad, swapped(out_grad), first, 1)
    stream_pair = jnp.concatenate(
        [stream_full, in_order(stream_there, swapped(stream_there), first, 1)], axis=0
    )
    out_pair = jnp.concatenate([out_full, in_order(out_there, swapped(out_there), first, 1)], axis=0)

    top_count = route_ids.shape[1]
    pair_ids, pair_weights = facts[:top_count].astype(jnp.int32), facts[top_count:]
    place = jnp.arange(2 * tok_rows, dtype=jnp.int32)
    block_of = place // tok_rows
    half_of = jnp.where(upper, 1 - block_of, block_of)

    def ranks(ids, expert_of, blocks):
        hit = ids[:, None, :] == expert_of[None, :, None]
        named = jnp.any(hit, axis=0)
        at = place[: blocks.shape[0]]
        before = (at[:, None] < at[None, :]) & (blocks[:, None] == blocks[None, :])
        rank = mm(named.astype(BF), before.astype(BF), ((1,), (0,)))
        return hit, jnp.where(named, rank.astype(jnp.int32) - tp * part, -1)

    slot_at = jnp.arange(part, dtype=jnp.int32)
    _, slot_home = ranks(route_ids.T, jnp.arange(experts, dtype=jnp.int32), block_of[:tok_rows])
    pick_home = (slot_home[:, None, :] == slot_at[None, :, None]).astype(BF).reshape(slots, tok_rows)
    here = jnp.arange(half_experts, dtype=jnp.int32) + jnp.where(upper, half_experts, 0)
    hit, slot_of = ranks(pair_ids, here, block_of)
    weight_of = jnp.sum(jnp.where(hit, pair_weights[:, None, :], 0.0), axis=0)
    chosen = (slot_of[:, None, None, :] == slot_at[None, None, :, None]) & (
        half_of[None, None, None, :] == jnp.arange(2, dtype=jnp.int32)[None, :, None, None]
    )
    pick = chosen.astype(BF).reshape(slots, 2 * tok_rows)
    slot_weight = jnp.sum(jnp.where(chosen, weight_of[:, None, None, :], 0.0), axis=3).reshape(slots, 1)

    half_groups = [[h * half + i for i in range(half)] for h in range(2)]
    send_rows = mm(pick, stream_pair, ((1,), (0,))).astype(BF)
    send_cot = (mm(pick, out_pair, ((1,), (0,))) * slot_weight).astype(BF)
    rows = exchanged(send_rows.reshape(half, 2 * part, width), half_groups).reshape(slots, width)
    cot = exchanged(send_cot.reshape(half, 2 * part, width), half_groups).reshape(slots, width)

    gate_all = jnp.concatenate([w_gate[0], swapped(w_gate[0])], axis=1)
    up_all = jnp.concatenate([w_up[0], swapped(w_up[0])], axis=1)
    down_all = jnp.concatenate([w_down[0], swapped(w_down[0])], axis=0)
    hid = w_gate.shape[2]

    pre_gate = mm(rows, gate_all, ((1,), (0,)))
    pre_up = mm(rows, up_all, ((1,), (0,)))
    sigmoid_gate = jax.nn.sigmoid(pre_gate)
    silu_gate = pre_gate * sigmoid_gate
    hidden = (silu_gate * pre_up).astype(BF)
    slope = pre_up * sigmoid_gate * (1.0 + pre_gate * (1.0 - sigmoid_gate))
    hidden, silu_gate, slope = lax.optimization_barrier((hidden, silu_gate, slope))
    both_all = jnp.concatenate([gate_all, up_all], axis=1)
    hidden_grad = mm(cot, down_all, ((1,), (1,)))
    up_grad = (hidden_grad * silu_gate).astype(BF)
    gate_grad = (hidden_grad * slope).astype(BF)
    both_grad = jnp.concatenate([gate_grad, up_grad], axis=1)
    row_grad = mm(both_grad, both_all, ((1,), (1,))).astype(BF)
    row_grad = jnp.transpose(row_grad.reshape(half, 2, part, width), (1, 0, 2, 3))
    back = exchanged(row_grad.reshape(experts, part, width)).reshape(slots, width)

    rows_both = jnp.concatenate([rows, swapped(rows)], axis=0)
    cot_both = jnp.concatenate([cot, swapped(cot)], axis=0)
    gate_both = jnp.concatenate([gate_grad[:, :hid], swapped(gate_grad[:, hid:])], axis=0)
    up_both = jnp.concatenate([up_grad[:, :hid], swapped(up_grad[:, hid:])], axis=0)
    hidden_both = jnp.concatenate([hidden[:, :hid], swapped(hidden[:, hid:])], axis=0)
    gate_w_grad = mm(rows_both, gate_both, ((0,), (0,)))
    up_w_grad = mm(rows_both, up_both, ((0,), (0,)))
    down_w_grad = mm(hidden_both, cot_both, ((0,), (0,)))

    mine = mm(pick_home, back, ((0,), (0,))).astype(BF)
    stream_whole = (
        out_full.astype(F32) + (mine.astype(F32) + swapped(mine).astype(F32))
    ).astype(BF)
    stream_half = jnp.where(first, stream_whole[:, :half_width], stream_whole[:, half_width:])

    depth = taps.shape[0]
    channels = conv_gate.shape[1]
    prod_rows = conv_gate.astype(F32) * conv_value.astype(F32)
    left_rows = passed_along(prod_rows[tok_rows - depth + 1 :], "sp", 1)
    padded = jnp.concatenate([left_rows, prod_rows], axis=0)
    conv_sum = jnp.zeros((tok_rows, channels), F32)
    for tap_index in range(depth):
        conv_sum = conv_sum + taps[tap_index][None, :] * padded[tap_index : tap_index + tok_rows]
    mixer_out = (gate_in.astype(F32) * conv_sum).astype(BF)

    mixer_grad = mm(stream_whole, w_out, ((1,), (0,))).astype(BF)
    mixer_wide = mixer_grad.astype(F32)
    gate_in_grad = (mixer_wide * conv_sum).astype(BF)
    conv_inner = mixer_wide * gate_in.astype(F32)
    right_rows = passed_along(conv_inner[: depth - 1], "sp", -1)
    padded_back = jnp.concatenate([conv_inner, right_rows], axis=0)
    prod_grad = jnp.zeros((tok_rows, channels), F32)
    for tap_index in range(depth):
        offset = depth - 1 - tap_index
        prod_grad = prod_grad + taps[tap_index][None, :] * padded_back[offset : offset + tok_rows]
    conv_gate_grad = (prod_grad * conv_value.astype(F32)).astype(BF)
    conv_value_grad = (prod_grad * conv_gate.astype(F32)).astype(BF)

    inner_count = 1 << ((sp_count.bit_length() - 1) // 2)
    outer_count = sp_count // inner_count
    inner = lax.rem(lax.axis_index("sp"), inner_count)

    def across(shard, step):
        return lax.ppermute(shard, "sp", [(i, i ^ step) for i in range(sp_count)])

    wide_mixer = jnp.concatenate([mixer_out] + [across(mixer_out, step) for step in range(1, inner_count)], axis=0)
    block = width // sp_count
    half_outer = outer_count // 2
    pieces = []
    for step in range(inner_count):
        piece = jnp.concatenate(
            [
                lax.dynamic_slice_in_dim(
                    stream_half, (o * inner_count + (inner ^ step)) * block, block, 1
                )
                for o in range(half_outer)
            ],
            axis=1,
        )
        pieces.append(across(piece, step) if step else piece)
    features = jnp.concatenate(pieces, axis=0)
    features = in_order(features, swapped(features), first, 1)
    partial = mm(features, wide_mixer, ((0,), (0,))).astype(BF).reshape(outer_count, block, channels)
    outer = lax.div(lax.axis_index("sp"), inner_count)
    out_proj_grad = lax.dynamic_index_in_dim(partial, outer, 0, keepdims=False).astype(F32)
    for step in range(outer_count - 1, 0, -1):
        piece = lax.dynamic_index_in_dim(partial, outer ^ step, 0, keepdims=False)
        piece = across(piece, step * inner_count)
        out_proj_grad = out_proj_grad + piece.astype(F32)

    return (
        stream_half,
        gate_in_grad,
        conv_gate_grad,
        conv_value_grad,
        out_proj_grad,
        gate_w_grad[None],
        up_w_grad[None],
        down_w_grad[None],
    )


def solution(mesh):
    placed = (
        P("sp", "tp"),
        P("sp", "tp"),
        P("sp", "tp"),
        P("sp", "tp"),
        P("sp", "tp"),
        P(None, "tp"),
        P(None, "tp"),
        P("sp", None),
        P("sp", None),
        P("sp", None, "tp"),
        P("sp", None, "tp"),
        P("sp", "tp", None),
    )
    return jax.shard_map(
        shards,
        mesh=mesh,
        in_specs=placed,
        out_specs=(
            P("sp", "tp"),
            P("sp", "tp"),
            P("sp", "tp"),
            P("sp", "tp"),
            P("sp", "tp"),
            P("sp", None, "tp"),
            P("sp", None, "tp"),
            P("sp", "tp", None),
        ),
        check_vma=False,
    )
```

profile of v0, /device:TPU:0, one launch (start us, length us, event | category | flops | bytes accessed | tf_op | source)
XLA Modules:
  0.0 248.0 jit_solution(2666643883297330152)
XLA Ops:
  0.6 4.1 %collective-permute-start.6 = (bf16[256,1024]{1,0:T(8,128)(2,1)}, bf16[256,1024]{1,0:T(8,128)(2,1)S(1)}, u32[]{:S(2)}, u32[]{:S(2)}) collective-permute-start(bf16[256,1024]{1,0:T(8,128)(2,1)} %param.12), channel_id=1, source_target_pairs={{0,16},{2,18},{4,20},{6,22},{8,24},{10,26},{12,28},{14,30},{16,0},... | collective-permute-start | bytes 1572872 | tf_op jit(solution)/shard_map/ppermute | solution.py:67
  6.4 21.9 %collective-permute-done.1 = f32[4,256]{1,0:T(4,128)S(1)} collective-permute-done((f32[4,256]{1,0:T(4,128)S(1)}, f32[4,256]{1,0:T(4,128)S(1)}, u32[]{:S(2)}, u32[]{:S(2)}) %collective-permute-start.1) | collective-permute-done | bytes 4128 | tf_op jit(solution)/shard_map/ppermute | solution.py:67
  34.7 4.5 %all-to-all-start.1 = ((bf16[8,64,2048]{2,1,0:T(8,128)(2,1)}), bf16[8,64,2048]{2,1,0:T(8,128)(2,1)}, u32[]{:S(2)}, u32[]{:S(2)}) async-start(bf16[8,64,2048]{2,1,0:T(8,128)(2,1)} %bitcast.49), calls=%async_computation.1 | async-start | bytes 4194304 | tf_op jit(solution)/shard_map/all_to_all | solution.py:21
  39.2 3.0 %collective-permute-start.2 = (bf16[256,1024]{1,0:T(8,128)(2,1)S(1)}, bf16[256,1024]{1,0:T(8,128)(2,1)}, u32[]{:S(2)}, u32[]{:S(2)}) collective-permute-start(bf16[256,1024]{1,0:T(8,128)(2,1)S(1)} %copy-done.11), channel_id=1, source_target_pairs={{0,16},{2,18},{4,20},{6,22},{8,24},{10,26},{12,28},{14,30},{16,0},... | collective-permute-start | bytes 1572872 | tf_op jit(solution)/shard_map/ppermute | solution.py:67
  42.1 31.9 %collective-permute-done.2 = bf16[256,1024]{1,0:T(8,128)(2,1)} collective-permute-done((bf16[256,1024]{1,0:T(8,128)(2,1)S(1)}, bf16[256,1024]{1,0:T(8,128)(2,1)}, u32[]{:S(2)}, u32[]{:S(2)}) %collective-permute-start.2) | collective-permute-done | bytes 524320 | tf_op jit(solution)/shard_map/ppermute | solution.py:67
  81.0 11.5 %all-to-all-start = ((bf16[8,64,2048]{2,1,0:T(8,128)(2,1)}), bf16[8,64,2048]{2,1,0:T(8,128)(2,1)}, u32[]{:S(2)}, u32[]{:S(2)}) async-start(bf16[8,64,2048]{2,1,0:T(8,128)(2,1)} %bitcast.50), calls=%async_computation | async-start | bytes 4194304 | tf_op jit(solution)/shard_map/all_to_all | solution.py:21
  93.2 3.6 %collective-permute-done.9 = bf16[2048,512]{1,0:T(8,128)(2,1)S(1)} collective-permute-done((bf16[2048,512]{1,0:T(8,128)(2,1)}, bf16[2048,512]{1,0:T(8,128)(2,1)S(1)}, u32[]{:S(2)}, u32[]{:S(2)}) %collective-permute-start.9) | collective-permute-done | bytes 2097184 | tf_op jit(solution)/shard_map/ppermute | solution.py:17
  96.9 5.4 %fusion.16 = f32[512,1024]{1,0:T(8,128)S(1)} fusion(bf16[512,2048]{1,0:T(8,128)(2,1)} %bitcast.7, bf16[2048,512]{1,0:T(8,128)(2,1)S(1)} %collective-permute-done.9, bf16[2048,512]{1,0:T(8,128)(2,1)} %bitcast.68), kind=kOutput, calls=%fused_computation.16 | convolution fusion | flops 2155872256 | bytes 8388608 | tf_op jit(solution)/shard_map/dot_general | solution.py:35
  102.3 7.3 %add_multiply_fusion = (f32[512,1024]{1,0:T(8,128)}, bf16[512,1024]{1,0:T(8,128)(2,1)}, f32[512,1024]{1,0:T(8,128)}) fusion(f32[512,1024]{1,0:T(8,128)S(1)} %fusion.16, bf16[512,2048]{1,0:T(8,128)(2,1)} %bitcast.7, bf16[2048,512]{1,0:T(8,128)(2,1)S(1)} %collective-permute-done.8, bf16[2048,512]{1,0:T(8,128)(2,1)S(1)} %bitcast.71), kind=kOutput, calls=%fused_computation.45 | convolution fusion | flops 2161639424 | bytes 13631488 | tf_op jit(solution)/shard_map/dot_general | solution.py:35
  109.6 9.5 %all-to-all-done = bf16[8,64,2048]{2,1,0:T(8,128)(2,1)} async-done(((bf16[8,64,2048]{2,1,0:T(8,128)(2,1)}), bf16[8,64,2048]{2,1,0:T(8,128)(2,1)}, u32[]{:S(2)}, u32[]{:S(2)}) %all-to-all-start) | async-done | bytes 2097184 | tf_op jit(solution)/shard_map/all_to_all | solution.py:21
  119.1 6.6 %multiply_convert_fusion.2 = (bf16[512,1024]{1,0:T(8,128)(2,1)S(1)}, bf16[512,1024]{1,0:T(8,128)(2,1)S(1)}) fusion(f32[512,1024]{1,0:T(8,128)} %get-tuple-element.11, f32[512,1024]{1,0:T(8,128)} %get-tuple-element.12, bf16[512,2048]{1,0:T(8,128)(2,1)} %bitcast.4, bf16[512,2048]{1,0:T(8,128)(2,1)} %collective-permute-done.4, bf16[512,2048]{1,0:T(8,128)(2,1)} %bitcast.66), kind=kOutput, calls=%fused_computation.44 | convolution fusion | flops 2157969408 | bytes 12582912 | tf_op jit(solution)/shard_map/dot_general | solution.py:35
  125.8 4.5 %fusion.27 = bf16[512,2048]{1,0:T(8,128)(2,1)S(1)} fusion(bf16[2048,512]{1,0:T(8,128)(2,1)S(1)} %copy-done.21, bf16[2048,512]{1,0:T(8,128)(2,1)S(1)} %bitcast.69, bf16[2048,512]{1,0:T(8,128)(2,1)S(1)} %copy-done.23, bf16[2048,512]{1,0:T(8,128)(2,1)S(1)} %bitcast.72, bf16[512,1024]{1,0:T(8,128)(2,1)S(1)} %get-tuple-element.21, ...), kind=kOutput, calls=%fused_computation.29 | convolution fusion | flops 4333764608 | bytes 12582912 | tf_op jit(solution)/shard_map/dot_general | solution.py:35
  131.8 6.5 %all-to-all-start.2 = ((bf16[16,32,2048]{2,1,0:T(8,128)(2,1)}), bf16[16,32,2048]{2,1,0:T(8,128)(2,1)}, u32[]{:S(2)}, u32[]{:S(2)}) async-start(bf16[16,32,2048]{2,1,0:T(8,128)(2,1)} %bitcast.48), calls=%async_computation.2 | async-start | bytes 4194304 | tf_op jit(solution)/shard_map/all_to_all | solution.py:21
  140.2 4.1 %collective-permute-start.11 = (f32[2,512]{1,0:T(2,128)S(1)}, f32[2,512]{1,0:T(2,128)S(1)}, u32[]{:S(2)}, u32[]{:S(2)}) collective-permute-start(f32[2,512]{1,0:T(2,128)S(1)} %slice.91), channel_id=1, source_target_pairs={{0,2},{2,4},{4,6},{6,8},{8,10},{10,12},{12,14},{14,16},{16,18},{18... | collective-permute-start | bytes 12296 | tf_op jit(solution)/shard_map/ppermute | solution.py:13
  145.4 2.6 %fusion.97 = (bf16[256,512]{1,0:T(8,128)(2,1)}, f32[256,512]{1,0:T(8,128)}) fusion(bf16[256,512]{1,0:T(8,128)(2,1)S(1)} %copy-done.8, f32[256,512]{1,0:T(8,128)} %copy-done.1, f32[512]{0:T(512)S(1)} %bitcast.58, f32[2,512]{1,0:T(2,128)S(1)} %collective-permute-done.11, f32[512]{0:T(512)S(1)} %bitcast.60, f32[512]{0:T(512)S(1)} %bitcast.56), kind=kLoop, calls=%fused_computation.124 | loop fusion | flops 1310720 | bytes 1583104 | tf_op jit(solution)/shard_map/convert_element_type | solution.py:156
  151.9 29.1 %all-to-all-done.2 = bf16[16,32,2048]{2,1,0:T(8,128)(2,1)} async-done(((bf16[16,32,2048]{2,1,0:T(8,128)(2,1)}), bf16[16,32,2048]{2,1,0:T(8,128)(2,1)}, u32[]{:S(2)}, u32[]{:S(2)}) %all-to-all-start.2) | async-done | bytes 2097184 | tf_op jit(solution)/shard_map/all_to_all | solution.py:21
  184.2 6.8 %convolution_bitcast_fusion.1 = f32[1,2048,512]{2,1,0:T(8,128)} fusion(bf16[512,2048]{1,0:T(8,128)(2,1)} %collective-permute-done.23, bf16[512,2048]{1,0:T(8,128)(2,1)} %bitcast.7, bf16[512,512]{1,0:T(8,128)(2,1)} %collective-permute-done.24, bf16[512,512]{1,0:T(8,128)(2,1)S(1)} %copy-done.13), kind=kOutput, calls=%fused_computation.28 | convolution fusion | flops 2157969408 | bytes 9437184 | tf_op jit(solution)/shard_map/dot_general | solution.py:35
  191.0 6.7 %convolution_bitcast_fusion = f32[1,2048,512]{2,1,0:T(8,128)} fusion(bf16[512,2048]{1,0:T(8,128)(2,1)} %collective-permute-done.23, bf16[512,2048]{1,0:T(8,128)(2,1)} %bitcast.7, bf16[512,512]{1,0:T(8,128)(2,1)} %collective-permute-done.25, bf16[512,512]{1,0:T(8,128)(2,1)S(1)} %copy-done.12), kind=kOutput, calls=%fused_computation.27 | convolution fusion | flops 2157969408 | bytes 9437184 | tf_op jit(solution)/shard_map/dot_general | solution.py:35
  198.5 3.3 %collective-permute-start.15 = (bf16[256,256]{1,0:T(8,128)(2,1)S(1)}, bf16[256,256]{1,0:T(8,128)(2,1)S(1)}, u32[]{:S(2)}, u32[]{:S(2)}) collective-permute-start(bf16[256,256]{1,0:T(8,128)(2,1)S(1)} %pad_maximum_fusion.8), channel_id=1, source_target_pairs={{0,6},{2,4},{4,2},{6,0},{8,14},{10,12},{12,10},{14,8},{16,22},{18,... | collective-permute-start | bytes 393224 | tf_op jit(solution)/shard_map/ppermute | solution.py:176
  205.7 3.4 %collective-permute-start.19 = (bf16[256,512]{1,0:T(8,128)(2,1)S(1)}, bf16[256,512]{1,0:T(8,128)(2,1)S(1)}, u32[]{:S(2)}, u32[]{:S(2)}) collective-permute-start(bf16[256,512]{1,0:T(8,128)(2,1)S(1)} %copy-done.14), channel_id=1, source_target_pairs={{0,6},{2,4},{4,2},{6,0},{8,14},{10,12},{12,10},{14,8},{16,22},{18,... | collective-permute-start | bytes 786440 | tf_op jit(solution)/shard_map/ppermute | solution.py:176
  213.1 6.7 %fusion.24 = f32[1,512,2048]{2,1,0:T(8,128)} fusion(bf16[512,2048]{1,0:T(8,128)(2,1)} %collective-permute-done.27, bf16[512,2048]{1,0:T(8,128)(2,1)} %bitcast.4, bf16[512,512]{1,0:T(8,128)(2,1)S(1)} %collective-permute-done.26, bf16[512,512]{1,0:T(8,128)(2,1)S(1)} %get-tuple-element.23), kind=kOutput, calls=%fused_computation.26 | convolution fusion | flops 2157969408 | bytes 9437184 | tf_op jit(solution)/shard_map/dot_general | solution.py:35
  222.7 8.8 %collective-permute-start.22 = (bf16[128,512]{1,0:T(8,128)(2,1)S(1)}, bf16[128,512]{1,0:T(8,128)(2,1)S(1)}, u32[]{:S(2)}, u32[]{:S(2)}) collective-permute-start(bf16[128,512]{1,0:T(8,128)(2,1)S(1)} %get-tuple-element.30), channel_id=1, source_target_pairs={{0,8},{2,10},{4,12},{6,14},{8,0},{10,2},{12,4},{14,6},{16,24},{18,... | collective-permute-start | bytes 393224 | tf_op jit(solution)/shard_map/ppermute | solution.py:176
  231.6 5.7 %collective-permute-start.21 = (bf16[128,512]{1,0:T(8,128)(2,1)S(1)}, bf16[128,512]{1,0:T(8,128)(2,1)S(1)}, u32[]{:S(2)}, u32[]{:S(2)}) collective-permute-start(bf16[128,512]{1,0:T(8,128)(2,1)S(1)} %get-tuple-element.31), channel_id=1, source_target_pairs={{0,16},{2,18},{4,20},{6,22},{8,24},{10,26},{12,28},{14,30},{16,0},... | collective-permute-start | bytes 393224 | tf_op jit(solution)/shard_map/ppermute | solution.py:176
  238.0 9.2 %collective-permute-done.21 = bf16[128,512]{1,0:T(8,128)(2,1)S(1)} collective-permute-done((bf16[128,512]{1,0:T(8,128)(2,1)S(1)}, bf16[128,512]{1,0:T(8,128)(2,1)S(1)}, u32[]{:S(2)}, u32[]{:S(2)}) %collective-permute-start.21) | collective-permute-done | bytes 131104 | tf_op jit(solution)/shard_map/ppermute | solution.py:176
  (141 shorter events, 40.0 us)
Async XLA Ops:
  0.6 28.8 %collective-permute-start.6 = (bf16[256,1024]{1,0:T(8,128)(2,1)}, bf16[256,1024]{1,0:T(8,128)(2,1)S(1)}, u32[]{:S(2)}, u32[]{:S(2)}) collective-permute-start(bf16[256,1024]{1,0:T(8,128)(2,1)} %param.12), channel_id=1, source_target_pairs={{0,16},{2,18},{4,20},{6,22},{8,24},{10,26},{12,28},{14,30},{16,0},... | collective-permute-start | bytes 1572872 | tf_op jit(solution)/shard_map/ppermute | solution.py:67
  4.8 25.0 %collective-permute-start.5 = (bf16[256,1024]{1,0:T(8,128)(2,1)}, bf16[256,1024]{1,0:T(8,128)(2,1)}, u32[]{:S(2)}, u32[]{:S(2)}) collective-permute-start(bf16[256,1024]{1,0:T(8,128)(2,1)} %param.12), channel_id=1, source_target_pairs={{0,1},{1,0},{2,3},{3,2},{4,5},{5,4},{6,7},{7,6},{8,9},{9,8},{10,11... | collective-permute-start | bytes 1572872 | tf_op jit(solution)/shard_map/ppermute | solution.py:17
  6.2 22.2 %collective-permute-start.1 = (f32[4,256]{1,0:T(4,128)S(1)}, f32[4,256]{1,0:T(4,128)S(1)}, u32[]{:S(2)}, u32[]{:S(2)}) collective-permute-start(f32[4,256]{1,0:T(4,128)S(1)} %pad_maximum_fusion.10), channel_id=1, source_target_pairs={{0,16},{2,18},{4,20},{6,22},{8,24},{10,26},{12,28},{14,30},{16,0},... | collective-permute-start | bytes 12296 | tf_op jit(solution)/shard_map/ppermute | solution.py:67
  34.7 46.3 %all-to-all-start.1 = ((bf16[8,64,2048]{2,1,0:T(8,128)(2,1)}), bf16[8,64,2048]{2,1,0:T(8,128)(2,1)}, u32[]{:S(2)}, u32[]{:S(2)}) async-start(bf16[8,64,2048]{2,1,0:T(8,128)(2,1)} %bitcast.49), calls=%async_computation.1 | async-start | bytes 4194304 | tf_op jit(solution)/shard_map/all_to_all | solution.py:21
  39.2 34.9 %collective-permute-start.2 = (bf16[256,1024]{1,0:T(8,128)(2,1)S(1)}, bf16[256,1024]{1,0:T(8,128)(2,1)}, u32[]{:S(2)}, u32[]{:S(2)}) collective-permute-start(bf16[256,1024]{1,0:T(8,128)(2,1)S(1)} %copy-done.11), channel_id=1, source_target_pairs={{0,16},{2,18},{4,20},{6,22},{8,24},{10,26},{12,28},{14,30},{16,0},... | collective-permute-start | bytes 1572872 | tf_op jit(solution)/shard_map/ppermute | solution.py:67
  42.1 32.3 %collective-permute-start = (bf16[256,1024]{1,0:T(8,128)(2,1)S(1)}, bf16[256,1024]{1,0:T(8,128)(2,1)}, u32[]{:S(2)}, u32[]{:S(2)}) collective-permute-start(bf16[256,1024]{1,0:T(8,128)(2,1)S(1)} %copy-done.11), channel_id=1, source_target_pairs={{0,1},{1,0},{2,3},{3,2},{4,5},{5,4},{6,7},{7,6},{8,9},{9,8},{10,11... | collective-permute-start | bytes 1572872 | tf_op jit(solution)/shard_map/ppermute | solution.py:17
  81.0 38.1 %all-to-all-start = ((bf16[8,64,2048]{2,1,0:T(8,128)(2,1)}), bf16[8,64,2048]{2,1,0:T(8,128)(2,1)}, u32[]{:S(2)}, u32[]{:S(2)}) async-start(bf16[8,64,2048]{2,1,0:T(8,128)(2,1)} %bitcast.50), calls=%async_computation | async-start | bytes 4194304 | tf_op jit(solution)/shard_map/all_to_all | solution.py:21
  92.7 9.5 %collective-permute-start.8 = (bf16[2048,512]{1,0:T(8,128)(2,1)}, bf16[2048,512]{1,0:T(8,128)(2,1)S(1)}, u32[]{:S(2)}, u32[]{:S(2)}) collective-permute-start(bf16[2048,512]{1,0:T(8,128)(2,1)} %bitcast.70), channel_id=1, source_target_pairs={{0,1},{1,0},{2,3},{3,2},{4,5},{5,4},{6,7},{7,6},{8,9},{9,8},{10,11... | collective-permute-start | bytes 6291464 | tf_op jit(solution)/shard_map/ppermute | solution.py:17
  93.0 16.6 %collective-permute-start.4 = (bf16[512,2048]{1,0:T(8,128)(2,1)}, bf16[512,2048]{1,0:T(8,128)(2,1)}, u32[]{:S(2)}, u32[]{:S(2)}) collective-permute-start(bf16[512,2048]{1,0:T(8,128)(2,1)} %bitcast.65), channel_id=1, source_target_pairs={{0,1},{1,0},{2,3},{3,2},{4,5},{5,4},{6,7},{7,6},{8,9},{9,8},{10,11... | collective-permute-start | bytes 6291464 | tf_op jit(solution)/shard_map/ppermute | solution.py:17
  131.8 49.2 %all-to-all-start.2 = ((bf16[16,32,2048]{2,1,0:T(8,128)(2,1)}), bf16[16,32,2048]{2,1,0:T(8,128)(2,1)}, u32[]{:S(2)}, u32[]{:S(2)}) async-start(bf16[16,32,2048]{2,1,0:T(8,128)(2,1)} %bitcast.48), calls=%async_computation.2 | async-start | bytes 4194304 | tf_op jit(solution)/shard_map/all_to_all | solution.py:21
  144.3 39.9 %collective-permute-start.23 = (bf16[512,2048]{1,0:T(8,128)(2,1)}, bf16[512,2048]{1,0:T(8,128)(2,1)}, u32[]{:S(2)}, u32[]{:S(2)}) collective-permute-start(bf16[512,2048]{1,0:T(8,128)(2,1)} %bitcast.7), channel_id=1, source_target_pairs={{0,1},{1,0},{2,3},{3,2},{4,5},{5,4},{6,7},{7,6},{8,9},{9,8},{10,11... | collective-permute-start | bytes 6291464 | tf_op jit(solution)/shard_map/ppermute | solution.py:17
  148.1 64.9 %collective-permute-start.27 = (bf16[512,2048]{1,0:T(8,128)(2,1)}, bf16[512,2048]{1,0:T(8,128)(2,1)}, u32[]{:S(2)}, u32[]{:S(2)}) collective-permute-start(bf16[512,2048]{1,0:T(8,128)(2,1)} %bitcast.4), channel_id=1, source_target_pairs={{0,1},{1,0},{2,3},{3,2},{4,5},{5,4},{6,7},{7,6},{8,9},{9,8},{10,11... | collective-permute-start | bytes 6291464 | tf_op jit(solution)/shard_map/ppermute | solution.py:17
  150.3 33.4 %collective-permute-start.24 = (bf16[512,512]{1,0:T(8,128)(2,1)}, bf16[512,512]{1,0:T(8,128)(2,1)}, u32[]{:S(2)}, u32[]{:S(2)}) collective-permute-start(bf16[512,512]{1,0:T(8,128)(2,1)} %get-tuple-element.28), channel_id=1, source_target_pairs={{0,1},{1,0},{2,3},{3,2},{4,5},{5,4},{6,7},{7,6},{8,9},{9,8},{10,11... | collective-permute-start | bytes 1572872 | tf_op jit(solution)/shard_map/ppermute | solution.py:17
  151.9 39.1 %collective-permute-start.25 = (bf16[512,512]{1,0:T(8,128)(2,1)}, bf16[512,512]{1,0:T(8,128)(2,1)}, u32[]{:S(2)}, u32[]{:S(2)}) collective-permute-start(bf16[512,512]{1,0:T(8,128)(2,1)} %get-tuple-element.26), channel_id=1, source_target_pairs={{0,1},{1,0},{2,3},{3,2},{4,5},{5,4},{6,7},{7,6},{8,9},{9,8},{10,11... | collective-permute-start | bytes 1572872 | tf_op jit(solution)/shard_map/ppermute | solution.py:17
  183.5 14.2 %collective-permute-start.10 = (bf16[256,2048]{1,0:T(8,128)(2,1)S(1)}, bf16[256,2048]{1,0:T(8,128)(2,1)S(1)}, u32[]{:S(2)}, u32[]{:S(2)}) collective-permute-start(bf16[256,2048]{1,0:T(8,128)(2,1)S(1)} %fusion.30), channel_id=1, source_target_pairs={{0,1},{1,0},{2,3},{3,2},{4,5},{5,4},{6,7},{7,6},{8,9},{9,8},{10,11... | collective-permute-start | bytes 3145736 | tf_op jit(solution)/shard_map/ppermute | solution.py:17
  183.7 28.0 %collective-permute-start.26 = (bf16[512,512]{1,0:T(8,128)(2,1)S(1)}, bf16[512,512]{1,0:T(8,128)(2,1)S(1)}, u32[]{:S(2)}, u32[]{:S(2)}) collective-permute-start(bf16[512,512]{1,0:T(8,128)(2,1)S(1)} %get-tuple-element.24), channel_id=1, source_target_pairs={{0,1},{1,0},{2,3},{3,2},{4,5},{5,4},{6,7},{7,6},{8,9},{9,8},{10,11... | collective-permute-start | bytes 1572872 | tf_op jit(solution)/shard_map/ppermute | solution.py:17
  205.7 16.2 %collective-permute-start.19 = (bf16[256,512]{1,0:T(8,128)(2,1)S(1)}, bf16[256,512]{1,0:T(8,128)(2,1)S(1)}, u32[]{:S(2)}, u32[]{:S(2)}) collective-permute-start(bf16[256,512]{1,0:T(8,128)(2,1)S(1)} %copy-done.14), channel_id=1, source_target_pairs={{0,6},{2,4},{4,2},{6,0},{8,14},{10,12},{12,10},{14,8},{16,22},{18,... | collective-permute-start | bytes 786440 | tf_op jit(solution)/shard_map/ppermute | solution.py:176
  209.1 12.8 %collective-permute-start.18 = (bf16[256,512]{1,0:T(8,128)(2,1)S(1)}, bf16[256,512]{1,0:T(8,128)(2,1)S(1)}, u32[]{:S(2)}, u32[]{:S(2)}) collective-permute-start(bf16[256,512]{1,0:T(8,128)(2,1)S(1)} %copy-done.14), channel_id=1, source_target_pairs={{0,4},{2,6},{4,0},{6,2},{8,12},{10,14},{12,8},{14,10},{16,20},{18,... | collective-permute-start | bytes 786440 | tf_op jit(solution)/shard_map/ppermute | solution.py:176
  210.3 11.7 %collective-permute-start.17 = (bf16[256,512]{1,0:T(8,128)(2,1)S(1)}, bf16[256,512]{1,0:T(8,128)(2,1)S(1)}, u32[]{:S(2)}, u32[]{:S(2)}) collective-permute-start(bf16[256,512]{1,0:T(8,128)(2,1)S(1)} %copy-done.14), channel_id=1, source_target_pairs={{0,2},{2,0},{4,6},{6,4},{8,10},{10,8},{12,14},{14,12},{16,18},{18,... | collective-permute-start | bytes 786440 | tf_op jit(solution)/shard_map/ppermute | solution.py:176
  211.7 9.3 %collective-permute-start.12 = (f32[2,512]{1,0:T(2,128)S(1)}, f32[2,512]{1,0:T(2,128)S(1)}, u32[]{:S(2)}, u32[]{:S(2)}) collective-permute-start(f32[2,512]{1,0:T(2,128)S(1)} %slice.94), channel_id=1, source_target_pairs={{2,0},{4,2},{6,4},{8,6},{10,8},{12,10},{14,12},{16,14},{18,16},{20... | collective-permute-start | bytes 12296 | tf_op jit(solution)/shard_map/ppermute | solution.py:13
  213.0 9.0 %collective-permute-start.16 = (bf16[1024,256]{1,0:T(8,128)(2,1)S(1)}, bf16[1024,256]{1,0:T(8,128)(2,1)S(1)}, u32[]{:S(2)}, u32[]{:S(2)}) collective-permute-start(bf16[1024,256]{1,0:T(8,128)(2,1)S(1)} %pad_maximum_fusion.5), channel_id=1, source_target_pairs={{0,1},{1,0},{2,3},{3,2},{4,5},{5,4},{6,7},{7,6},{8,9},{9,8},{10,11... | collective-permute-start | bytes 1572872 | tf_op jit(solution)/shard_map/ppermute | solution.py:17
  222.7 15.3 %collective-permute-start.22 = (bf16[128,512]{1,0:T(8,128)(2,1)S(1)}, bf16[128,512]{1,0:T(8,128)(2,1)S(1)}, u32[]{:S(2)}, u32[]{:S(2)}) collective-permute-start(bf16[128,512]{1,0:T(8,128)(2,1)S(1)} %get-tuple-element.30), channel_id=1, source_target_pairs={{0,8},{2,10},{4,12},{6,14},{8,0},{10,2},{12,4},{14,6},{16,24},{18,... | collective-permute-start | bytes 393224 | tf_op jit(solution)/shard_map/ppermute | solution.py:176
  231.6 15.6 %collective-permute-start.21 = (bf16[128,512]{1,0:T(8,128)(2,1)S(1)}, bf16[128,512]{1,0:T(8,128)(2,1)S(1)}, u32[]{:S(2)}, u32[]{:S(2)}) collective-permute-start(bf16[128,512]{1,0:T(8,128)(2,1)S(1)} %get-tuple-element.31), channel_id=1, source_target_pairs={{0,16},{2,18},{4,20},{6,22},{8,24},{10,26},{12,28},{14,30},{16,0},... | collective-permute-start | bytes 393224 | tf_op jit(solution)/shard_map/ppermute | solution.py:176
  237.2 10.0 %collective-permute-start.20 = (bf16[128,512]{1,0:T(8,128)(2,1)S(1)}, bf16[128,512]{1,0:T(8,128)(2,1)S(1)}, u32[]{:S(2)}, u32[]{:S(2)}) collective-permute-start(bf16[128,512]{1,0:T(8,128)(2,1)S(1)} %get-tuple-element.29), channel_id=1, source_target_pairs={{0,24},{2,26},{4,28},{6,30},{8,16},{10,18},{12,20},{14,22},{16,8},... | collective-permute-start | bytes 393224 | tf_op jit(solution)/shard_map/ppermute | solution.py:176
  (31 other events, 394.4 us)
where the time goes:
time: 249 us; the launch traced here: 248 us
  waiting for transfers between devices  108 us (43%)
  starting transfers between devices  62.8 us (25%)
  matrix products  54.3 us (22%)
  other arithmetic  15.7 us (6%)
  local copies, waits for them, and re-layouts  6.01 us (2%)
    dot_general x14, matrix products, mm(): lax.dot_general(left, right, (dims, ((), ())), preferred_element_type=F32)  54.3 us
    ppermute x3, waiting for transfers between devices, traded(): return lax.ppermute(shard, 'sp', [(i, i ^ half) for i in range(sp_count)])  53.8 us
    all_to_all x3, waiting for transfers between devices, exchanged(): lax.all_to_all(blocks, 'sp', split_axis=0, concat_axis=0, tiled=True, axi...  38.6 us
    ppermute x9, starting transfers between devices, across(): return lax.ppermute(shard, 'sp', [(i, i ^ step) for i in range(sp_count)])  25.5 us
    all_to_all x3, starting transfers between devices, exchanged(): lax.all_to_all(blocks, 'sp', split_axis=0, concat_axis=0, tiled=True, axi...  22.5 us
    ppermute x9, waiting for transfers between devices, across(): return lax.ppermute(shard, 'sp', [(i, i ^ step) for i in range(sp_count)])  9.92 us
    ppermute x3, starting transfers between devices, traded(): return lax.ppermute(shard, 'sp', [(i, i ^ half) for i in range(sp_count)])  7.31 us
    select_n x4, other arithmetic, in_order(): jnp.where(first, jnp.concatenate([mine, other], axis=axis), jnp.concatena...  6.18 us
  transfers between devices with their start and end apart: 31, of which 9 were waited for; matrix products, arithmetic and copies ran while one was open for 23% of the time, Pallas kernels for 0%

commit v1 on v0

--- a/solution.py
+++ b/solution.py
@@ -1,6 +1,9 @@
+import functools
 import jax
 import jax.numpy as jnp
 from jax import lax
+from jax.experimental import pallas as pl
+from jax.experimental.pallas import tpu as pltpu
 from jax.sharding import PartitionSpec as P
 
 BF = jnp.bfloat16
@@ -33,6 +36,114 @@
 
 def mm(left, right, dims):
     return lax.dot_general(left, right, (dims, ((), ())), preferred_element_type=F32)
+
+
+def back_kernel(first_steps, half_outer, inner_count, part, cot, down, silu, slope, gate, up, gate_grad, up_grad, row_grad):
+    step = pl.program_id(0)
+    tile = silu.shape[1]
+
+    @pl.when(step < first_steps)
+    def _():
+        hidden_grad = mm(cot[...], down[...], ((1,), (1,)))
+        at = pl.ds(pl.multiple_of(step * tile, tile), tile)
+        gate_grad[:, at] = (hidden_grad * slope[...]).astype(BF)
+        up_grad[:, at] = (hidden_grad * silu[...]).astype(BF)
+
+    @pl.when(step >= first_steps)
+    def _():
+        cut, units = gate.shape[0] * gate.shape[2], gate.shape[3]
+        rows = mm(gate_grad[...], gate[...].reshape(cut, units), ((1,), (1,)))
+        rows += mm(up_grad[...], up[...].reshape(cut, units), ((1,), (1,)))
+        for h in range(2):
+            for o in range(half_outer):
+                picked = []
+                for i in range(inner_count):
+                    at = ((o * inner_count + i) * 2 + h) * part
+                    picked.append(rows[at : at + part])
+                row_grad[h * half_outer + o, 0] = jnp.concatenate(picked, axis=0).astype(BF)
+
+
+def row_grads(cot, down, silu, slope, gate, up, outer_count, inner_count, part):
+    slots, width = cot.shape
+    units = down.shape[0]
+    tile, cut = min(units, 512), width // inner_count
+    block = cut // outer_count
+    first_steps = units // tile
+
+    def early(i):
+        return jnp.minimum(i, first_steps - 1)
+
+    def late(i):
+        return jnp.maximum(i - first_steps, 0)
+
+    by_group = (outer_count, inner_count, block, units)
+    kept = pl.BlockSpec((slots, units), lambda i: (0, 0))
+    cols = pl.BlockSpec((slots, tile), lambda i: (0, early(i)))
+    group = pl.BlockSpec((outer_count, 1, block, units), lambda i: (0, late(i), 0, 0))
+    return pl.pallas_call(
+        functools.partial(back_kernel, first_steps, outer_count // 2, inner_count, part),
+        grid=(first_steps + inner_count,),
+        in_specs=[
+            pl.BlockSpec((slots, width), lambda i: (0, 0)),
+            pl.BlockSpec((tile, width), lambda i: (early(i), 0)),
+            cols,
+            cols,
+            group,
+            group,
+        ],
+        out_specs=[
+            kept,
+            kept,
+            pl.BlockSpec((outer_count, 1, inner_count * part, cut), lambda i: (0, late(i), 0, 0)),
+        ],
+        out_shape=[
+            jax.ShapeDtypeStruct((slots, units), BF),
+            jax.ShapeDtypeStruct((slots, units), BF),
+            jax.ShapeDtypeStruct((outer_count, inner_count, inner_count * part, cut), BF),
+        ],
+        compiler_params=pltpu.CompilerParams(vmem_limit_bytes=62 * 2**20),
+        cost_estimate=pl.CostEstimate(
+            flops=6 * slots * width * units, bytes_accessed=8 * width * units, transcendentals=0
+        ),
+        name="row_grads",
+    )(cot, down, silu, slope, gate.reshape(by_group), up.reshape(by_group))
+
+
+def home_kernel(inner, pick, back, mine):
+    tok_rows = pick.shape[0] // back.shape[1]
+    experts, inner_count, part, cut = back.shape
+    for j in range(inner_count):
+        rows = back[:, inner[0] ^ j].astype(F32).reshape(experts * part, cut).astype(BF)
+        at = slice(j * tok_rows, (j + 1) * tok_rows)
+        mine[at] = mm(pick[at], rows, ((1,), (0,))).astype(BF)
+
+
+def add_kernel(core, out_cut, mine, other, stream_cut, own_half):
+    total = out_cut[...].astype(F32) + (mine[...].astype(F32) + other[...].astype(F32))
+    total = total.astype(BF)
+    stream_cut[...] = total
+    wide = own_half.shape[1]
+    own_half[...] = jnp.where(core[0] == 0, total[:, :wide], total[:, wide:])
+
+
+def place_kernel(inner, block, *refs):
+    pieces, out = refs[:-1], refs[-1]
+    count = len(pieces)
+    for j, piece in enumerate(pieces):
+        for o in range(piece.shape[1] // block):
+            at = pl.multiple_of((o * count + (inner[0] ^ j)) * block, block)
+            out[:, pl.ds(at, block)] = piece[:, o * block : (o + 1) * block]
+
+
+def local_kernel(kernel, shapes, scalar, *arrays):
+    vmem = pl.BlockSpec(memory_space=pltpu.MemorySpace.VMEM)
+    return pl.pallas_call(
+        kernel,
+        in_specs=[pl.BlockSpec(memory_space=pltpu.MemorySpace.SMEM)] + [vmem] * len(arrays),
+        out_specs=[vmem] * len(shapes),
+        out_shape=[jax.ShapeDtypeStruct(shape, BF) for shape in shapes],
+        compiler_params=pltpu.CompilerParams(vmem_limit_bytes=24 * 2**20),
+    )(scalar.astype(jnp.int32).reshape(1), *arrays)
 
 
 def shards(
@@ -59,6 +170,16 @@
     tp = lax.axis_index("tp")
     first = tp == 0
 
+    inner_count = 1 << ((sp_count.bit_length() - 1) // 2)
+    outer_count = sp_count // inner_count
+    inner = lax.rem(lax.axis_index("sp"), inner_count)
+
+    def across(shard, step):
+        return lax.ppermute(shard, "sp", [(i, i ^ step) for i in range(sp_count)])
+
+    block = width // sp_count
+    half_outer = outer_count // 2
+
     half = sp_count // 2
     half_experts = experts // 2
     upper = lax.axis_index("sp") >= half
@@ -83,19 +204,16 @@
     block_of = place // tok_rows
     half_of = jnp.where(upper, 1 - block_of, block_of)
 
-    def ranks(ids, expert_of, blocks):
+    def ranks(ids, expert_of, blocks, at):
         hit = ids[:, None, :] == expert_of[None, :, None]
         named = jnp.any(hit, axis=0)
-        at = place[: blocks.shape[0]]
         before = (at[:, None] < at[None, :]) & (blocks[:, None] == blocks[None, :])
         rank = mm(named.astype(BF), before.astype(BF), ((1,), (0,)))
         return hit, jnp.where(named, rank.astype(jnp.int32) - tp * part, -1)
 
     slot_at = jnp.arange(part, dtype=jnp.int32)
-    _, slot_home = ranks(route_ids.T, jnp.arange(experts, dtype=jnp.int32), block_of[:tok_rows])
-    pick_home = (slot_home[:, None, :] == slot_at[None, :, None]).astype(BF).reshape(slots, tok_rows)
     here = jnp.arange(half_experts, dtype=jnp.int32) + jnp.where(upper, half_experts, 0)
-    hit, slot_of = ranks(pair_ids, here, block_of)
+    hit, slot_of = ranks(pair_ids, here, block_of, place)
     weight_of = jnp.sum(jnp.where(hit, pair_weights[:, None, :], 0.0), axis=0)
     chosen = (slot_of[:, None, None, :] == slot_at[None, None, :, None]) & (
         half_of[None, None, None, :] == jnp.arange(2, dtype=jnp.int32)[None, :, None, None]
@@ -108,42 +226,6 @@
     send_cot = (mm(pick, out_pair, ((1,), (0,))) * slot_weight).astype(BF)
     rows = exchanged(send_rows.reshape(half, 2 * part, width), half_groups).reshape(slots, width)
     cot = exchanged(send_cot.reshape(half, 2 * part, width), half_groups).reshape(slots, width)
-
-    gate_all = jnp.concatenate([w_gate[0], swapped(w_gate[0])], axis=1)
-    up_all = jnp.concatenate([w_up[0], swapped(w_up[0])], axis=1)
-    down_all = jnp.concatenate([w_down[0], swapped(w_down[0])], axis=0)
-    hid = w_gate.shape[2]
-
-    pre_gate = mm(rows, gate_all, ((1,), (0,)))
-    pre_up = mm(rows, up_all, ((1,), (0,)))
-    sigmoid_gate = jax.nn.sigmoid(pre_gate)
-    silu_gate = pre_gate * sigmoid_gate
-    hidden = (silu_gate * pre_up).astype(BF)
-    slope = pre_up * sigmoid_gate * (1.0 + pre_gate * (1.0 - sigmoid_gate))
-    hidden, silu_gate, slope = lax.optimization_barrier((hidden, silu_gate, slope))
-    both_all = jnp.concatenate([gate_all, up_all], axis=1)
-    hidden_grad = mm(cot, down_all, ((1,), (1,)))
-    up_grad = (hidden_grad * silu_gate).astype(BF)
-    gate_grad = (hidden_grad * slope).astype(BF)
-    both_grad = jnp.concatenate([gate_grad, up_grad], axis=1)
-    row_grad = mm(both_grad, both_all, ((1,), (1,))).astype(BF)
-    row_grad = jnp.transpose(row_grad.reshape(half, 2, part, width), (1, 0, 2, 3))
-    back = exchanged(row_grad.reshape(experts, part, width)).reshape(slots, width)
-
-    rows_both = jnp.concatenate([rows, swapped(rows)], axis=0)
-    cot_both = jnp.concatenate([cot, swapped(cot)], axis=0)
-    gate_both = jnp.concatenate([gate_grad[:, :hid], swapped(gate_grad[:, hid:])], axis=0)
-    up_both = jnp.concatenate([up_grad[:, :hid], swapped(up_grad[:, hid:])], axis=0)
-    hidden_both = jnp.concatenate([hidden[:, :hid], swapped(hidden[:, hid:])], axis=0)
-    gate_w_grad = mm(rows_both, gate_both, ((0,), (0,)))
-    up_w_grad = mm(rows_both, up_both, ((0,), (0,)))
-    down_w_grad = mm(hidden_both, cot_both, ((0,), (0,)))
-
-    mine = mm(pick_home, back, ((0,), (0,))).astype(BF)
-    stream_whole = (
-        out_full.astype(F32) + (mine.astype(F32) + swapped(mine).astype(F32))
-    ).astype(BF)
-    stream_half = jnp.where(first, stream_whole[:, :half_width], stream_whole[:, half_width:])
 
     depth = taps.shape[0]
     channels = conv_gate.shape[1]
@@ -154,6 +236,85 @@
     for tap_index in range(depth):
         conv_sum = conv_sum + taps[tap_index][None, :] * padded[tap_index : tap_index + tok_rows]
     mixer_out = (gate_in.astype(F32) * conv_sum).astype(BF)
+
+    wide_mixer, out_cut, group_ids = [mixer_out], [], [route_ids.T.astype(F32)]
+    for step in range(inner_count):
+        piece = jnp.concatenate(
+            [
+                lax.dynamic_slice_in_dim(out_grad, (o * inner_count + (inner ^ step)) * block, block, 1)
+                for o in range(half_outer)
+            ],
+            axis=1,
+        )
+        if step:
+            group_ids.append(across(group_ids[0], step))
+            piece = across(piece, step)
+            wide_mixer.append(across(mixer_out, step))
+        out_cut.append(piece)
+    wide_mixer = jnp.concatenate(wide_mixer, axis=0)
+    group_ids = jnp.concatenate(group_ids, axis=1).astype(jnp.int32)
+    out_cut = jnp.concatenate(out_cut, axis=0)
+    out_cut = in_order(out_cut, swapped(out_cut), first, 1)
+    group_place = jnp.arange(inner_count * tok_rows, dtype=jnp.int32)
+    group_block = group_place // tok_rows
+    _, slot_group = ranks(group_ids, jnp.arange(experts, dtype=jnp.int32), group_block, group_place)
+    pick_group = (slot_group[:, None, :] == slot_at[None, :, None]).astype(BF)
+    pick_group = pick_group.reshape(slots, inner_count * tok_rows).T
+
+    gate_swap, up_swap, down_swap = swapped(w_gate[0]), swapped(w_up[0]), swapped(w_down[0])
+    gate_all = jnp.concatenate([w_gate[0], gate_swap], axis=1)
+    up_all = jnp.concatenate([w_up[0], up_swap], axis=1)
+    down_all = jnp.concatenate([w_down[0], down_swap], axis=0)
+    hid = w_gate.shape[2]
+
+    pre_gate = mm(rows, gate_all, ((1,), (0,)))
+    pre_up = mm(rows, up_all, ((1,), (0,)))
+    sigmoid_gate = jax.nn.sigmoid(pre_gate)
+    silu_gate = pre_gate * sigmoid_gate
+    hidden = (silu_gate * pre_up).astype(BF)
+    slope = pre_up * sigmoid_gate * (1.0 + pre_gate * (1.0 - sigmoid_gate))
+    hidden, silu_gate, slope = lax.optimization_barrier((hidden, silu_gate, slope))
+    cut = width // inner_count
+    gate_grad, up_grad, row_grad = row_grads(
+        cot, down_all, silu_gate, slope, gate_all, up_all, outer_count, inner_count, part
+    )
+    back = exchanged(row_grad.reshape(sp_count, inner_count * part, cut))
+
+    rows_both = jnp.concatenate([rows, swapped(rows)], axis=0)
+    cot_both = jnp.concatenate([cot, swapped(cot)], axis=0)
+    gate_both = jnp.concatenate([gate_grad[:, :hid], swapped(gate_grad[:, hid:])], axis=0)
+    up_both = jnp.concatenate([up_grad[:, :hid], swapped(up_grad[:, hid:])], axis=0)
+    hidden_both = jnp.concatenate([hidden[:, :hid], swapped(hidden[:, hid:])], axis=0)
+    gate_w_grad = mm(rows_both, gate_both, ((0,), (0,)))
+    up_w_grad = mm(rows_both, up_both, ((0,), (0,)))
+    down_w_grad = mm(hidden_both, cot_both, ((0,), (0,)))
+
+    group_tokens = inner_count * tok_rows
+    core_half = half_outer * block
+    (mine,) = local_kernel(
+        home_kernel, [(group_tokens, cut)], inner, pick_group,
+        back.reshape(experts, inner_count, part, cut),
+    )
+    stream_cut, own_half = local_kernel(
+        add_kernel, [(group_tokens, cut), (group_tokens, core_half)], tp,
+        out_cut, mine, swapped(mine),
+    )
+    pieces = [own_half[:tok_rows]]
+    for step in range(1, inner_count):
+        pieces.append(across(own_half[step * tok_rows : (step + 1) * tok_rows], step))
+    if block % 128 == 0:
+        (stream_half,) = local_kernel(
+            lambda inner_ref, *refs: place_kernel(inner_ref, block, *refs),
+            [(tok_rows, half_width)], inner, *pieces,
+        )
+    else:
+        pieces = jnp.stack(pieces)
+        ordered = [lax.dynamic_index_in_dim(pieces, inner ^ i, 0, keepdims=False) for i in range(inner_count)]
+        stream_half = jnp.concatenate(
+            [ordered[i][:, o * block : (o + 1) * block] for o in range(half_outer) for i in range(inner_count)],
+            axis=1,
+        )
+    stream_whole = in_order(stream_half, swapped(stream_half), first, 1)
 
     mixer_grad = mm(stream_whole, w_out, ((1,), (0,))).astype(BF)
     mixer_wide = mixer_grad.astype(F32)
@@ -168,31 +329,7 @@
     conv_gate_grad = (prod_grad * conv_value.astype(F32)).astype(BF)
     conv_value_grad = (prod_grad * conv_gate.astype(F32)).astype(BF)
 
-    inner_count = 1 << ((sp_count.bit_length() - 1) // 2)
-    outer_count = sp_count // inner_count
-    inner = lax.rem(lax.axis_index("sp"), inner_count)
-
-    def across(shard, step):
-        return lax.ppermute(shard, "sp", [(i, i ^ step) for i in range(sp_count)])
-
-    wide_mixer = jnp.concatenate([mixer_out] + [across(mixer_out, step) for step in range(1, inner_count)], axis=0)
-    block = width // sp_count
-    half_outer = outer_count // 2
-    pieces = []
-    for step in range(inner_count):
-        piece = jnp.concatenate(
-            [
-                lax.dynamic_slice_in_dim(
-                    stream_half, (o * inner_count + (inner ^ step)) * block, block, 1
-                )
-                for o in range(half_outer)
-            ],
-            axis=1,
-        )
-        pieces.append(across(piece, step) if step else piece)
-    features = jnp.concatenate(pieces, axis=0)
-    features = in_order(features, swapped(features), first, 1)
-    partial = mm(features, wide_mixer, ((0,), (0,))).astype(BF).reshape(outer_count, block, channels)
+    partial = mm(stream_cut, wide_mixer, ((0,), (0,))).astype(BF).reshape(outer_count, block, channels)
     outer = lax.div(lax.axis_index("sp"), inner_count)
     out_proj_grad = lax.dynamic_index_in_dim(partial, outer, 0, keepdims=False).astype(F32)
     for step in range(outer_count - 1, 0, -1):

time: 249 us -> 247 us (level)
  waiting for transfers between devices: 108 us -> 74.3 us
  other arithmetic: 15.7 us -> 38.4 us
  matrix products: 54.3 us -> 38.1 us
  Pallas kernels: 0 us -> 15.8 us
  starting transfers between devices: 62.8 us -> 67.2 us
  local copies, waits for them, and re-layouts: 6.01 us -> 10.4 us
    all_to_all x3, waiting for transfers between devices: 38.6 us -> 3.83 us  [exchanged(): lax.all_to_all(blocks, 'sp', split_axis=0, concat_axis=0, tiled=True, axi...]
    concatenate x4 -> x7, other arithmetic: 0.09 us -> 16.7 us  [the longest x1 4.99 us: shards(): gate_all = jnp.concatenate([w_gate[0], gate_swap], axis=1)]
    dot_general x14 -> x11, matrix products: 54.3 us -> 38.1 us  [mm(): lax.dot_general(left, right, (dims, ((), ())), preferred_element_type=F32)]
    pallas_call x0 -> x4, Pallas kernels: none -> 15.8 us  [the longest x1 13.7 us: row_grads(): pl.pallas_call(functools.partial(back_kernel, first_steps, outer_count //...]
    ppermute x9 -> x15, waiting for transfers between devices: 9.92 us -> 15.6 us  [across(): return lax.ppermute(shard, 'sp', [(i, i ^ step) for i in range(sp_count)])]
    eq x0 -> x4, local copies, waits for them, and re-layouts: none -> 5.13 us  [shards(): pick_group = (slot_group[:, None, :] == slot_at[None, :, None]).astype(BF)]
    ppermute x9 -> x15, starting transfers between devices: 25.5 us -> 30 us  [across(): return lax.ppermute(shard, 'sp', [(i, i ^ step) for i in range(sp_count)])]
    select_n x4 -> x5, other arithmetic: 6.18 us -> 10.5 us  [in_order(): jnp.where(first, jnp.concatenate([mine, other], axis=axis), jnp.concatena...]
  transfers between devices with their start and end apart: 31 -> 38, of which waited for: 9 -> 10; matrix products, arithmetic and copies ran while one was open for 23% -> 32% of each run, Pallas kernels for 0% -> 1%
where the time goes in v1:
time: 247 us; the launch traced here: 245 us
  waiting for transfers between devices  74.3 us (30%)
  starting transfers between devices  67.2 us (27%)
  other arithmetic  38.4 us (16%)
  matrix products  38.1 us (15%)
  Pallas kernels  15.8 us (6%)
  local copies, waits for them, and re-layouts  10.4 us (4%)
    ppermute x3, waiting for transfers between devices, traded(): return lax.ppermute(shard, 'sp', [(i, i ^ half) for i in range(sp_count)])  53.3 us
    dot_general x11, matrix products, mm(): lax.dot_general(left, right, (dims, ((), ())), preferred_element_type=F32)  38.1 us
    ppermute x15, starting transfers between devices, across(): return lax.ppermute(shard, 'sp', [(i, i ^ step) for i in range(sp_count)])  30 us
    all_to_all x3, starting transfers between devices, exchanged(): lax.all_to_all(blocks, 'sp', split_axis=0, concat_axis=0, tiled=True, axi...  22 us
    ppermute x15, waiting for transfers between devices, across(): return lax.ppermute(shard, 'sp', [(i, i ^ step) for i in range(sp_count)])  15.6 us
    pallas_call x1, Pallas kernels, row_grads(): pl.pallas_call(functools.partial(back_kernel, first_steps, outer_count //...  13.7 us
    select_n x5, other arithmetic, in_order(): jnp.where(first, jnp.concatenate([mine, other], axis=axis), jnp.concatena...  10.5 us
    ppermute x3, starting transfers between devices, traded(): return lax.ppermute(shard, 'sp', [(i, i ^ half) for i in range(sp_count)])  7.61 us
  transfers between devices with their start and end apart: 38, of which 10 were waited for; matrix products, arithmetic and copies ran while one was open for 32% of the time, Pallas kernels for 1%

profile of v1, /device:TPU:0, one launch (start us, length us, event | category | flops | bytes accessed | tf_op | source)
XLA Modules:
  0.0 245.4 jit_solution(3631676580821926377)
XLA Ops:
  0.6 4.1 %collective-permute-start.13 = (bf16[256,1024]{1,0:T(8,128)(2,1)}, bf16[256,1024]{1,0:T(8,128)(2,1)S(1)}, u32[]{:S(2)}, u32[]{:S(2)}) collective-permute-start(bf16[256,1024]{1,0:T(8,128)(2,1)} %param.12), channel_id=1, source_target_pairs={{0,16},{2,18},{4,20},{6,22},{8,24},{10,26},{12,28},{14,30},{16,0},... | collective-permute-start | bytes 1572872 | tf_op jit(solution)/shard_map/ppermute | solution.py:188
  6.3 22.0 %collective-permute-done.7 = f32[4,256]{1,0:T(4,128)S(1)} collective-permute-done((f32[4,256]{1,0:T(4,128)S(1)}, f32[4,256]{1,0:T(4,128)S(1)}, u32[]{:S(2)}, u32[]{:S(2)}) %collective-permute-start.7) | collective-permute-done | bytes 4128 | tf_op jit(solution)/shard_map/ppermute | solution.py:188
  34.4 4.1 %all-to-all-start.1 = ((bf16[8,64,2048]{2,1,0:T(8,128)(2,1)}), bf16[8,64,2048]{2,1,0:T(8,128)(2,1)S(1)}, u32[]{:S(2)}, u32[]{:S(2)}) async-start(bf16[8,64,2048]{2,1,0:T(8,128)(2,1)} %bitcast.57), calls=%async_computation.1 | async-start | bytes 4194304 | tf_op jit(solution)/shard_map/all_to_all | solution.py:24
  38.5 3.4 %collective-permute-start.9 = (bf16[256,1024]{1,0:T(8,128)(2,1)S(1)}, bf16[256,1024]{1,0:T(8,128)(2,1)S(1)}, u32[]{:S(2)}, u32[]{:S(2)}) collective-permute-start(bf16[256,1024]{1,0:T(8,128)(2,1)S(1)} %copy-done.1), channel_id=1, source_target_pairs={{0,16},{2,18},{4,20},{6,22},{8,24},{10,26},{12,28},{14,30},{16,0},... | collective-permute-start | bytes 1572872 | tf_op jit(solution)/shard_map/ppermute | solution.py:188
  41.9 31.2 %collective-permute-done.9 = bf16[256,1024]{1,0:T(8,128)(2,1)S(1)} collective-permute-done((bf16[256,1024]{1,0:T(8,128)(2,1)S(1)}, bf16[256,1024]{1,0:T(8,128)(2,1)S(1)}, u32[]{:S(2)}, u32[]{:S(2)}) %collective-permute-start.9) | collective-permute-done | bytes 524320 | tf_op jit(solution)/shard_map/ppermute | solution.py:188
  81.1 12.1 %all-to-all-start = ((bf16[8,64,2048]{2,1,0:T(8,128)(2,1)}), bf16[8,64,2048]{2,1,0:T(8,128)(2,1)}, u32[]{:S(2)}, u32[]{:S(2)}) async-start(bf16[8,64,2048]{2,1,0:T(8,128)(2,1)} %bitcast.58), calls=%async_computation | async-start | bytes 4194304 | tf_op jit(solution)/shard_map/all_to_all | solution.py:24
  93.2 5.0 %pad_maximum_fusion.1.gate = bf16[4,4,128,1024]{3,2,1,0:T(8,128)(2,1)} fusion(bf16[4,4,128,512]{3,2,1,0:T(8,128)(2,1)} %bitcast.15, bf16[4,4,128,512]{3,2,1,0:T(8,128)(2,1)} %bitcast.65), kind=kLoop, calls=%fused_computation.9 | loop fusion | flops 8388608 | bytes 8388608 | tf_op jit(solution)/shard_map/concatenate | solution.py:265
  98.2 4.4 %pad_maximum_fusion.2.up = bf16[4,4,128,1024]{3,2,1,0:T(8,128)(2,1)} fusion(bf16[4,4,128,512]{3,2,1,0:T(8,128)(2,1)} %bitcast.17, bf16[4,4,128,512]{3,2,1,0:T(8,128)(2,1)S(1)} %bitcast.62), kind=kLoop, calls=%fused_computation.10 | loop fusion | flops 8388608 | bytes 8388608 | tf_op jit(solution)/shard_map/concatenate | solution.py:266
  102.5 4.2 %pad_maximum_fusion.down = bf16[1024,2048]{1,0:T(8,128)(2,1)} fusion(bf16[512,2048]{1,0:T(8,128)(2,1)} %collective-permute-done.11, bf16[512,2048]{1,0:T(8,128)(2,1)S(1)} %bitcast.60), kind=kLoop, calls=%fused_computation | loop fusion | flops 8388608 | bytes 8388608 | tf_op jit(solution)/shard_map/concatenate | solution.py:267
  106.7 4.1 %fusion.4 = f32[512,1024]{1,0:T(8,128)S(1)} fusion(bf16[512,2048]{1,0:T(8,128)(2,1)S(1)} %bitcast.51, bf16[2048,512]{1,0:T(8,128)(2,1)} %collective-permute-done.16, bf16[2048,512]{1,0:T(8,128)(2,1)S(1)} %bitcast.63), kind=kOutput, calls=%fused_computation.5 | convolution fusion | flops 2155872256 | bytes 8388608 | tf_op jit(solution)/shard_map/dot_general | solution.py:38
  110.8 7.0 %add_multiply_fusion = (f32[512,1024]{1,0:T(8,128)}, bf16[512,1024]{1,0:T(8,128)(2,1)}, f32[512,1024]{1,0:T(8,128)}) fusion(f32[512,1024]{1,0:T(8,128)S(1)} %fusion.4, bf16[512,2048]{1,0:T(8,128)(2,1)S(1)} %bitcast.52, bf16[2048,512]{1,0:T(8,128)(2,1)} %collective-permute-done.15, bf16[2048,512]{1,0:T(8,128)(2,1)S(1)} %bitcast.66), kind=kOutput, calls=%fused_computation.30 | convolution fusion | flops 2161639424 | bytes 13631488 | tf_op jit(solution)/shard_map/dot_general | solution.py:38
  119.3 13.7 %row_grads.1 = (bf16[512,1024]{1,0:T(8,128)(2,1)}, bf16[512,1024]{1,0:T(8,128)(2,1)}, bf16[4,4,128,512]{3,2,1,0:T(8,128)(2,1)}) custom-call(bf16[512,2048]{1,0:T(8,128)(2,1)} %bitcast.8.cot, bf16[1024,2048]{1,0:T(8,128)(2,1)} %pad_maximum_fusion.down, f32[512,1024]{1,0:T(8,128)} %get-tuple-element.16.silu, f32[512,1024]{1,0:T(8,128)} %get-tuple-element.17.slope, ...), custom_call_target="tpu_custom_call" | custom-call | flops 6442450944 | bytes 16777216 | tf_op jit(solution)/shard_map/row_grads/pallas_call | solution.py:83
  133.0 5.8 %all-to-all-start.2 = ((bf16[16,128,512]{2,1,0:T(8,128)(2,1)}), bf16[16,128,512]{2,1,0:T(8,128)(2,1)S(1)}, u32[]{:S(2)}, u32[]{:S(2)}) async-start(bf16[16,128,512]{2,1,0:T(8,128)(2,1)} %bitcast.56), calls=%async_computation.2 | async-start | bytes 4194304 | tf_op jit(solution)/shard_map/all_to_all | solution.py:24
  150.3 6.4 %collective-permute-done.5 = f32[2,256]{1,0:T(2,128)} collective-permute-done((f32[2,256]{1,0:T(2,128)S(1)}, f32[2,256]{1,0:T(2,128)}, u32[]{:S(2)}, u32[]{:S(2)}) %collective-permute-start.5) | collective-permute-done | bytes 2080 | tf_op jit(solution)/shard_map/ppermute | solution.py:178
  156.7 4.0 %collective-permute-start.22 = (f32[2,512]{1,0:T(2,128)}, f32[2,512]{1,0:T(2,128)}, u32[]{:S(2)}, u32[]{:S(2)}) collective-permute-start(f32[2,512]{1,0:T(2,128)} %slice.89), channel_id=1, source_target_pairs={{0,2},{2,4},{4,6},{6,8},{8,10},{10,12},{12,14},{14,16},{16,18},{18... | collective-permute-start | bytes 12296 | tf_op jit(solution)/shard_map/ppermute | solution.py:16
  173.9 5.2 %maximum_select_fusion.out_cut = bf16[1024,512]{1,0:T(8,128)(2,1)S(1)} fusion(bf16[1024,256]{1,0:T(8,128)(2,1)S(1)} %collective-permute-done.3, bf16[256,256]{1,0:T(8,128)(2,1)S(1)} %copy-done.16, bf16[256,256]{1,0:T(8,128)(2,1)S(1)} %copy-done.18, bf16[256,256]{1,0:T(8,128)(2,1)S(1)} %copy-done.20, bf16[256,128]{1,0:T(8,128)(2,1)S(1)} %get-tuple-element.53, ...), kind=kLoop, calls=%fused_computation.47 | loop fusion | flops 13107200 | bytes 2097153 | tf_op jit(solution)/shard_map/jit(_where)/select_n | solution.py:30
  187.0 6.0 %convolution_bitcast_fusion.1 = f32[1,2048,512]{2,1,0:T(8,128)} fusion(bf16[512,2048]{1,0:T(8,128)(2,1)} %collective-permute-done.30, bf16[512,2048]{1,0:T(8,128)(2,1)S(1)} %bitcast.54, bf16[512,512]{1,0:T(8,128)(2,1)S(1)} %collective-permute-done.31, bf16[512,512]{1,0:T(8,128)(2,1)S(1)} %get-tuple-element.35), kind=kOutput, calls=%fused_computation.22 | convolution fusion | flops 2157969408 | bytes 9437184 | tf_op jit(solution)/shard_map/dot_general | solution.py:38
  194.7 3.3 %collective-permute-start.19 = (bf16[256,256]{1,0:T(8,128)(2,1)S(1)}, bf16[256,256]{1,0:T(8,128)(2,1)S(1)}, u32[]{:S(2)}, u32[]{:S(2)}) collective-permute-start(bf16[256,256]{1,0:T(8,128)(2,1)S(1)} %get-tuple-element.43), channel_id=1, source_target_pairs={{0,4},{2,6},{4,0},{6,2},{8,12},{10,14},{12,8},{14,10},{16,20},{18,... | collective-permute-start | bytes 393224 | tf_op jit(solution)/shard_map/ppermute | solution.py:178
  198.4 6.0 %convolution_bitcast_fusion = f32[1,2048,512]{2,1,0:T(8,128)} fusion(bf16[512,2048]{1,0:T(8,128)(2,1)} %collective-permute-done.30, bf16[512,2048]{1,0:T(8,128)(2,1)S(1)} %bitcast.55, bf16[512,512]{1,0:T(8,128)(2,1)S(1)} %collective-permute-done.32, bf16[512,512]{1,0:T(8,128)(2,1)S(1)} %get-tuple-element.33), kind=kOutput, calls=%fused_computation.21 | convolution fusion | flops 2157969408 | bytes 9437184 | tf_op jit(solution)/shard_map/dot_general | solution.py:38
  209.0 6.6 %fusion.15 = f32[1,512,2048]{2,1,0:T(8,128)} fusion(bf16[512,2048]{1,0:T(8,128)(2,1)} %collective-permute-done.34, bf16[512,2048]{1,0:T(8,128)(2,1)} %bitcast.8.cot, bf16[512,512]{1,0:T(8,128)(2,1)S(1)} %collective-permute-done.33, bf16[512,512]{1,0:T(8,128)(2,1)S(1)} %get-tuple-element.31), kind=kOutput, calls=%fused_computation.20 | convolution fusion | flops 2157969408 | bytes 9437184 | tf_op jit(solution)/shard_map/dot_general | solution.py:38
  215.6 3.4 %collective-permute-done.25 = bf16[256,512]{1,0:T(8,128)(2,1)S(1)} collective-permute-done((bf16[256,512]{1,0:T(8,128)(2,1)S(1)}, bf16[256,512]{1,0:T(8,128)(2,1)S(1)}, u32[]{:S(2)}, u32[]{:S(2)}) %collective-permute-start.25) | collective-permute-done | bytes 262176 | tf_op jit(solution)/shard_map/ppermute | solution.py:178
  220.1 9.9 %collective-permute-start.29 = (bf16[128,512]{1,0:T(8,128)(2,1)S(1)}, bf16[128,512]{1,0:T(8,128)(2,1)S(1)}, u32[]{:S(2)}, u32[]{:S(2)}) collective-permute-start(bf16[128,512]{1,0:T(8,128)(2,1)S(1)} %get-tuple-element.38), channel_id=1, source_target_pairs={{0,8},{2,10},{4,12},{6,14},{8,0},{10,2},{12,4},{14,6},{16,24},{18,... | collective-permute-start | bytes 393224 | tf_op jit(solution)/shard_map/ppermute | solution.py:178
  230.0 3.2 %collective-permute-start.28 = (bf16[128,512]{1,0:T(8,128)(2,1)S(1)}, bf16[128,512]{1,0:T(8,128)(2,1)S(1)}, u32[]{:S(2)}, u32[]{:S(2)}) collective-permute-start(bf16[128,512]{1,0:T(8,128)(2,1)S(1)} %get-tuple-element.39), channel_id=1, source_target_pairs={{0,16},{2,18},{4,20},{6,22},{8,24},{10,26},{12,28},{14,30},{16,0},... | collective-permute-start | bytes 393224 | tf_op jit(solution)/shard_map/ppermute | solution.py:178
  237.6 5.3 %collective-permute-done.27 = bf16[128,512]{1,0:T(8,128)(2,1)S(1)} collective-permute-done((bf16[128,512]{1,0:T(8,128)(2,1)S(1)}, bf16[128,512]{1,0:T(8,128)(2,1)S(1)}, u32[]{:S(2)}, u32[]{:S(2)}) %collective-permute-start.27) | collective-permute-done | bytes 131104 | tf_op jit(solution)/shard_map/ppermute | solution.py:178
  (168 shorter events, 63.7 us)
Async XLA Ops:
  0.6 28.8 %collective-permute-start.13 = (bf16[256,1024]{1,0:T(8,128)(2,1)}, bf16[256,1024]{1,0:T(8,128)(2,1)S(1)}, u32[]{:S(2)}, u32[]{:S(2)}) collective-permute-start(bf16[256,1024]{1,0:T(8,128)(2,1)} %param.12), channel_id=1, source_target_pairs={{0,16},{2,18},{4,20},{6,22},{8,24},{10,26},{12,28},{14,30},{16,0},... | collective-permute-start | bytes 1572872 | tf_op jit(solution)/shard_map/ppermute | solution.py:188
  4.8 25.0 %collective-permute-start.12 = (bf16[256,1024]{1,0:T(8,128)(2,1)}, bf16[256,1024]{1,0:T(8,128)(2,1)S(1)}, u32[]{:S(2)}, u32[]{:S(2)}) collective-permute-start(bf16[256,1024]{1,0:T(8,128)(2,1)} %param.12), channel_id=1, source_target_pairs={{0,1},{1,0},{2,3},{3,2},{4,5},{5,4},{6,7},{7,6},{8,9},{9,8},{10,11... | collective-permute-start | bytes 1572872 | tf_op jit(solution)/shard_map/ppermute | solution.py:20
  6.1 22.2 %collective-permute-start.7 = (f32[4,256]{1,0:T(4,128)S(1)}, f32[4,256]{1,0:T(4,128)S(1)}, u32[]{:S(2)}, u32[]{:S(2)}) collective-permute-start(f32[4,256]{1,0:T(4,128)S(1)} %pad_maximum_fusion.13), channel_id=1, source_target_pairs={{0,16},{2,18},{4,20},{6,22},{8,24},{10,26},{12,28},{14,30},{16,0},... | collective-permute-start | bytes 12296 | tf_op jit(solution)/shard_map/ppermute | solution.py:188
  34.4 46.7 %all-to-all-start.1 = ((bf16[8,64,2048]{2,1,0:T(8,128)(2,1)}), bf16[8,64,2048]{2,1,0:T(8,128)(2,1)S(1)}, u32[]{:S(2)}, u32[]{:S(2)}) async-start(bf16[8,64,2048]{2,1,0:T(8,128)(2,1)} %bitcast.57), calls=%async_computation.1 | async-start | bytes 4194304 | tf_op jit(solution)/shard_map/all_to_all | solution.py:24
  38.5 34.6 %collective-permute-start.9 = (bf16[256,1024]{1,0:T(8,128)(2,1)S(1)}, bf16[256,1024]{1,0:T(8,128)(2,1)S(1)}, u32[]{:S(2)}, u32[]{:S(2)}) collective-permute-start(bf16[256,1024]{1,0:T(8,128)(2,1)S(1)} %copy-done.1), channel_id=1, source_target_pairs={{0,16},{2,18},{4,20},{6,22},{8,24},{10,26},{12,28},{14,30},{16,0},... | collective-permute-start | bytes 1572872 | tf_op jit(solution)/shard_map/ppermute | solution.py:188
  41.9 33.3 %collective-permute-start.8 = (bf16[256,1024]{1,0:T(8,128)(2,1)S(1)}, bf16[256,1024]{1,0:T(8,128)(2,1)}, u32[]{:S(2)}, u32[]{:S(2)}) collective-permute-start(bf16[256,1024]{1,0:T(8,128)(2,1)S(1)} %copy-done.1), channel_id=1, source_target_pairs={{0,1},{1,0},{2,3},{3,2},{4,5},{5,4},{6,7},{7,6},{8,9},{9,8},{10,11... | collective-permute-start | bytes 1572872 | tf_op jit(solution)/shard_map/ppermute | solution.py:20
  73.1 29.5 %collective-permute-start.11 = (bf16[512,2048]{1,0:T(8,128)(2,1)}, bf16[512,2048]{1,0:T(8,128)(2,1)}, u32[]{:S(2)}, u32[]{:S(2)}) collective-permute-start(bf16[512,2048]{1,0:T(8,128)(2,1)} %bitcast.59), channel_id=1, source_target_pairs={{0,1},{1,0},{2,3},{3,2},{4,5},{5,4},{6,7},{7,6},{8,9},{9,8},{10,11... | collective-permute-start | bytes 6291464 | tf_op jit(solution)/shard_map/ppermute | solution.py:20
  73.6 24.6 %collective-permute-start.16 = (bf16[2048,512]{1,0:T(8,128)(2,1)}, bf16[2048,512]{1,0:T(8,128)(2,1)}, u32[]{:S(2)}, u32[]{:S(2)}) collective-permute-start(bf16[2048,512]{1,0:T(8,128)(2,1)} %bitcast.61), channel_id=1, source_target_pairs={{0,1},{1,0},{2,3},{3,2},{4,5},{5,4},{6,7},{7,6},{8,9},{9,8},{10,11... | collective-permute-start | bytes 6291464 | tf_op jit(solution)/shard_map/ppermute | solution.py:20
  73.6 19.6 %collective-permute-start.15 = (bf16[2048,512]{1,0:T(8,128)(2,1)}, bf16[2048,512]{1,0:T(8,128)(2,1)}, u32[]{:S(2)}, u32[]{:S(2)}) collective-permute-start(bf16[2048,512]{1,0:T(8,128)(2,1)} %bitcast.64), channel_id=1, source_target_pairs={{0,1},{1,0},{2,3},{3,2},{4,5},{5,4},{6,7},{7,6},{8,9},{9,8},{10,11... | collective-permute-start | bytes 6291464 | tf_op jit(solution)/shard_map/ppermute | solution.py:20
  81.1 38.2 %all-to-all-start = ((bf16[8,64,2048]{2,1,0:T(8,128)(2,1)}), bf16[8,64,2048]{2,1,0:T(8,128)(2,1)}, u32[]{:S(2)}, u32[]{:S(2)}) async-start(bf16[8,64,2048]{2,1,0:T(8,128)(2,1)} %bitcast.58), calls=%async_computation | async-start | bytes 4194304 | tf_op jit(solution)/shard_map/all_to_all | solution.py:24
  133.0 48.4 %all-to-all-start.2 = ((bf16[16,128,512]{2,1,0:T(8,128)(2,1)}), bf16[16,128,512]{2,1,0:T(8,128)(2,1)S(1)}, u32[]{:S(2)}, u32[]{:S(2)}) async-start(bf16[16,128,512]{2,1,0:T(8,128)(2,1)} %bitcast.56), calls=%async_computation.2 | async-start | bytes 4194304 | tf_op jit(solution)/shard_map/all_to_all | solution.py:24
  141.7 15.0 %collective-permute-start.5 = (f32[2,256]{1,0:T(2,128)S(1)}, f32[2,256]{1,0:T(2,128)}, u32[]{:S(2)}, u32[]{:S(2)}) collective-permute-start(f32[2,256]{1,0:T(2,128)S(1)} %convert_bitcast_fusion), channel_id=1, source_target_pairs={{0,4},{2,6},{4,0},{6,2},{8,12},{10,14},{12,8},{14,10},{16,20},{18,... | collective-permute-start | bytes 6152 | tf_op jit(solution)/shard_map/ppermute | solution.py:178
  142.3 18.5 %collective-permute-start.4 = (f32[2,256]{1,0:T(2,128)S(1)}, f32[2,256]{1,0:T(2,128)}, u32[]{:S(2)}, u32[]{:S(2)}) collective-permute-start(f32[2,256]{1,0:T(2,128)S(1)} %convert_bitcast_fusion), channel_id=1, source_target_pairs={{0,2},{2,0},{4,6},{6,4},{8,10},{10,8},{12,14},{14,12},{16,18},{18,... | collective-permute-start | bytes 6152 | tf_op jit(solution)/shard_map/ppermute | solution.py:178
  143.2 23.4 %collective-permute-start.2 = (bf16[256,256]{1,0:T(8,128)(2,1)}, bf16[256,256]{1,0:T(8,128)(2,1)S(1)}, u32[]{:S(2)}, u32[]{:S(2)}) collective-permute-start(bf16[256,256]{1,0:T(8,128)(2,1)} %pad_maximum_fusion.11), channel_id=1, source_target_pairs={{0,6},{2,4},{4,2},{6,0},{8,14},{10,12},{12,10},{14,8},{16,22},{18,... | collective-permute-start | bytes 393224 | tf_op jit(solution)/shard_map/ppermute | solution.py:178
  146.7 20.0 %collective-permute-start.1 = (bf16[256,256]{1,0:T(8,128)(2,1)}, bf16[256,256]{1,0:T(8,128)(2,1)S(1)}, u32[]{:S(2)}, u32[]{:S(2)}) collective-permute-start(bf16[256,256]{1,0:T(8,128)(2,1)} %pad_maximum_fusion.10), channel_id=1, source_target_pairs={{0,4},{2,6},{4,0},{6,2},{8,12},{10,14},{12,8},{14,10},{16,20},{18,... | collective-permute-start | bytes 393224 | tf_op jit(solution)/shard_map/ppermute | solution.py:178
  150.1 16.6 %collective-permute-start = (bf16[256,256]{1,0:T(8,128)(2,1)}, bf16[256,256]{1,0:T(8,128)(2,1)S(1)}, u32[]{:S(2)}, u32[]{:S(2)}) collective-permute-start(bf16[256,256]{1,0:T(8,128)(2,1)} %pad_maximum_fusion.9), channel_id=1, source_target_pairs={{0,2},{2,0},{4,6},{6,4},{8,10},{10,8},{12,14},{14,12},{16,18},{18,... | collective-permute-start | bytes 393224 | tf_op jit(solution)/shard_map/ppermute | solution.py:178
  156.7 15.2 %collective-permute-start.22 = (f32[2,512]{1,0:T(2,128)}, f32[2,512]{1,0:T(2,128)}, u32[]{:S(2)}, u32[]{:S(2)}) collective-permute-start(f32[2,512]{1,0:T(2,128)} %slice.89), channel_id=1, source_target_pairs={{0,2},{2,4},{4,6},{6,8},{8,10},{10,12},{12,14},{14,16},{16,18},{18... | collective-permute-start | bytes 12296 | tf_op jit(solution)/shard_map/ppermute | solution.py:16
  161.4 25.6 %collective-permute-start.30 = (bf16[512,2048]{1,0:T(8,128)(2,1)}, bf16[512,2048]{1,0:T(8,128)(2,1)}, u32[]{:S(2)}, u32[]{:S(2)}) collective-permute-start(bf16[512,2048]{1,0:T(8,128)(2,1)} %bitcast.53), channel_id=1, source_target_pairs={{0,1},{1,0},{2,3},{3,2},{4,5},{5,4},{6,7},{7,6},{8,9},{9,8},{10,11... | collective-permute-start | bytes 6291464 | tf_op jit(solution)/shard_map/ppermute | solution.py:20
  173.8 35.2 %collective-permute-start.34 = (bf16[512,2048]{1,0:T(8,128)(2,1)}, bf16[512,2048]{1,0:T(8,128)(2,1)}, u32[]{:S(2)}, u32[]{:S(2)}) collective-permute-start(bf16[512,2048]{1,0:T(8,128)(2,1)} %bitcast.8.cot), channel_id=1, source_target_pairs={{0,1},{1,0},{2,3},{3,2},{4,5},{5,4},{6,7},{7,6},{8,9},{9,8},{10,11... | collective-permute-start | bytes 6291464 | tf_op jit(solution)/shard_map/ppermute | solution.py:20
  184.8 13.2 %collective-permute-start.32 = (bf16[512,512]{1,0:T(8,128)(2,1)S(1)}, bf16[512,512]{1,0:T(8,128)(2,1)S(1)}, u32[]{:S(2)}, u32[]{:S(2)}) collective-permute-start(bf16[512,512]{1,0:T(8,128)(2,1)S(1)} %get-tuple-element.34), channel_id=1, source_target_pairs={{0,1},{1,0},{2,3},{3,2},{4,5},{5,4},{6,7},{7,6},{8,9},{9,8},{10,11... | collective-permute-start | bytes 1572872 | tf_op jit(solution)/shard_map/ppermute | solution.py:20
  186.9 22.1 %collective-permute-start.33 = (bf16[512,512]{1,0:T(8,128)(2,1)S(1)}, bf16[512,512]{1,0:T(8,128)(2,1)S(1)}, u32[]{:S(2)}, u32[]{:S(2)}) collective-permute-start(bf16[512,512]{1,0:T(8,128)(2,1)S(1)} %get-tuple-element.32), channel_id=1, source_target_pairs={{0,1},{1,0},{2,3},{3,2},{4,5},{5,4},{6,7},{7,6},{8,9},{9,8},{10,11... | collective-permute-start | bytes 1572872 | tf_op jit(solution)/shard_map/ppermute | solution.py:20
  207.0 12.3 %collective-permute-start.24 = (bf16[256,512]{1,0:T(8,128)(2,1)S(1)}, bf16[256,512]{1,0:T(8,128)(2,1)S(1)}, u32[]{:S(2)}, u32[]{:S(2)}) collective-permute-start(bf16[256,512]{1,0:T(8,128)(2,1)S(1)} %copy-done.23), channel_id=1, source_target_pairs={{0,2},{2,0},{4,6},{6,4},{8,10},{10,8},{12,14},{14,12},{16,18},{18,... | collective-permute-start | bytes 786440 | tf_op jit(solution)/shard_map/ppermute | solution.py:178
  209.0 25.7 %collective-permute-start.21 = (bf16[256,1024]{1,0:T(8,128)(2,1)}, bf16[256,1024]{1,0:T(8,128)(2,1)S(1)}, u32[]{:S(2)}, u32[]{:S(2)}) collective-permute-start(bf16[256,1024]{1,0:T(8,128)(2,1)} %shard_map.181), channel_id=1, source_target_pairs={{0,1},{1,0},{2,3},{3,2},{4,5},{5,4},{6,7},{7,6},{8,9},{9,8},{10,11... | collective-permute-start | bytes 1572872 | tf_op jit(solution)/shard_map/ppermute | solution.py:20
  220.1 17.4 %collective-permute-start.29 = (bf16[128,512]{1,0:T(8,128)(2,1)S(1)}, bf16[128,512]{1,0:T(8,128)(2,1)S(1)}, u32[]{:S(2)}, u32[]{:S(2)}) collective-permute-start(bf16[128,512]{1,0:T(8,128)(2,1)S(1)} %get-tuple-element.38), channel_id=1, source_target_pairs={{0,8},{2,10},{4,12},{6,14},{8,0},{10,2},{12,4},{14,6},{16,24},{18,... | collective-permute-start | bytes 393224 | tf_op jit(solution)/shard_map/ppermute | solution.py:178
  (41 other events, 330.3 us)

commit v2 on v1

--- a/solution.py
+++ b/solution.py
@@ -135,6 +135,14 @@
             out[:, pl.ds(at, block)] = piece[:, o * block : (o + 1) * block]
 
 
+def deal_kernel(core, pick, mine, other, there, there_other, dealt):
+    tok_rows, wide = mine.shape
+    own, far = pick[:, :tok_rows], pick[:, tok_rows:]
+    for at, near_rows, far_rows in ((core[0], mine, there), (1 - core[0], other, there_other)):
+        rows = mm(own, near_rows[...], ((1,), (0,))) + mm(far, far_rows[...], ((1,), (0,)))
+        dealt[:, pl.ds(pl.multiple_of(at * wide, 128), wide)] = rows.astype(BF)
+
+
 def local_kernel(kernel, shapes, scalar, *arrays):
     vmem = pl.BlockSpec(memory_space=pltpu.MemorySpace.VMEM)
     return pl.pallas_call(
@@ -191,11 +199,8 @@
     facts = jnp.concatenate([facts, traded(facts)], axis=1)
     stream_there = traded(stream)
     out_there = traded(out_grad)
-    stream_full = in_order(stream, swapped(stream), first, 1)
+    stream_other, stream_there_other = swapped(stream), swapped(stream_there)
     out_full = in_order(out_grad, swapped(out_grad), first, 1)
-    stream_pair = jnp.concatenate(
-        [stream_full, in_order(stream_there, swapped(stream_there), first, 1)], axis=0
-    )
     out_pair = jnp.concatenate([out_full, in_order(out_there, swapped(out_there), first, 1)], axis=0)
 
     top_count = route_ids.shape[1]
@@ -222,7 +227,10 @@
     slot_weight = jnp.sum(jnp.where(chosen, weight_of[:, None, None, :], 0.0), axis=3).reshape(slots, 1)
 
     half_groups = [[h * half + i for i in range(half)] for h in range(2)]
-    send_rows = mm(pick, stream_pair, ((1,), (0,))).astype(BF)
+    (send_rows,) = local_kernel(
+        deal_kernel, [(slots, width)], tp,
+        pick, stream, stream_other, stream_there, stream_there_other,
+    )
     send_cot = (mm(pick, out_pair, ((1,), (0,))) * slot_weight).astype(BF)
     rows = exchanged(send_rows.reshape(half, 2 * part, width), half_groups).reshape(slots, width)
     cot = exchanged(send_cot.reshape(half, 2 * part, width), half_groups).reshape(slots, width)
@@ -314,13 +322,20 @@
             [ordered[i][:, o * block : (o + 1) * block] for o in range(half_outer) for i in range(inner_count)],
             axis=1,
         )
-    stream_whole = in_order(stream_half, swapped(stream_half), first, 1)
-
-    mixer_grad = mm(stream_whole, w_out, ((1,), (0,))).astype(BF)
+    half_other = swapped(stream_half)
+    low, high = w_out[:half_width], w_out[half_width:]
+    w_mine, w_far = jnp.where(first, low, high), jnp.where(first, high, low)
+
+    top = min(tok_rows, 16)
+    first_grad = mm(stream_half[:top], w_mine, ((1,), (0,)))
+    first_grad = (first_grad + mm(half_other[:top], w_far, ((1,), (0,)))).astype(BF)
+    first_inner = first_grad.astype(F32) * gate_in[:top].astype(F32)
+    right_rows = passed_along(first_inner[: depth - 1], "sp", -1)
+    mixer_grad = mm(stream_half, w_mine, ((1,), (0,)))
+    mixer_grad = (mixer_grad + mm(half_other, w_far, ((1,), (0,)))).astype(BF)
     mixer_wide = mixer_grad.astype(F32)
     gate_in_grad = (mixer_wide * conv_sum).astype(BF)
     conv_inner = mixer_wide * gate_in.astype(F32)
-    right_rows = passed_along(conv_inner[: depth - 1], "sp", -1)
     padded_back = jnp.concatenate([conv_inner, right_rows], axis=0)
     prod_grad = jnp.zeros((tok_rows, channels), F32)
     for tap_index in range(depth):

time: 247 us -> 246 us (level)
  waiting for transfers between devices: 74.3 us -> 69.1 us
  starting transfers between devices: 67.2 us -> 72 us
  Pallas kernels: 15.8 us -> 18.3 us
    ppermute x15, waiting for transfers between devices: 15.6 us -> 9.88 us  [across(): return lax.ppermute(shard, 'sp', [(i, i ^ step) for i in range(sp_count)])]
    ppermute x15, starting transfers between devices: 30 us -> 34.5 us  [across(): return lax.ppermute(shard, 'sp', [(i, i ^ step) for i in range(sp_count)])]
    pallas_call x3 -> x4, Pallas kernels: 2.12 us -> 4.7 us  [local_kernel(): pl.pallas_call(kernel, in_specs=[pl.BlockSpec(memory_space=pltpu.MemorySp...]
    ppermute x2, waiting for transfers between devices: 0.01 us -> 2.57 us  [passed_along(): return lax.ppermute(shard, axis, pairs)]
    select_n x5 -> x3, other arithmetic: 10.5 us -> 8.54 us  [in_order(): jnp.where(first, jnp.concatenate([mine, other], axis=axis), jnp.concatena...]
    dot_general x11 -> x13, matrix products: 38.1 us -> 36.5 us  [mm(): lax.dot_general(left, right, (dims, ((), ())), preferred_element_type=F32)]
  transfers between devices with their start and end apart: 38 -> 38, of which waited for: 10 -> 8; matrix products, arithmetic and copies ran while one was open for 32% -> 33% of each run, Pallas kernels for 1% -> 1%
where the time goes in v2:
time: 246 us; the launch traced here: 245 us
  starting transfers between devices  72 us (29%)
  waiting for transfers between devices  69.1 us (28%)
  other arithmetic  36.6 us (15%)
  matrix products  36.5 us (15%)
  Pallas kernels  18.3 us (7%)
  local copies, waits for them, and re-layouts  11.3 us (5%)
    ppermute x3, waiting for transfers between devices, traded(): return lax.ppermute(shard, 'sp', [(i, i ^ half) for i in range(sp_count)])  53.6 us
    dot_general x13, matrix products, mm(): lax.dot_general(left, right, (dims, ((), ())), preferred_element_type=F32)  36.5 us
    ppermute x15, starting transfers between devices, across(): return lax.ppermute(shard, 'sp', [(i, i ^ step) for i in range(sp_count)])  34.5 us
    all_to_all x3, starting transfers between devices, exchanged(): lax.all_to_all(blocks, 'sp', split_axis=0, concat_axis=0, tiled=True, axi...  21.6 us
    pallas_call x1, Pallas kernels, row_grads(): pl.pallas_call(functools.partial(back_kernel, first_steps, outer_count //...  13.6 us
    ppermute x15, waiting for transfers between devices, across(): return lax.ppermute(shard, 'sp', [(i, i ^ step) for i in range(sp_count)])  9.88 us
    select_n x3, other arithmetic, in_order(): jnp.where(first, jnp.concatenate([mine, other], axis=axis), jnp.concatena...  8.54 us
    ppermute x3, starting transfers between devices, traded(): return lax.ppermute(shard, 'sp', [(i, i ^ half) for i in range(sp_count)])  7.05 us
  transfers between devices with their start and end apart: 38, of which 8 were waited for; matrix products, arithmetic and copies ran while one was open for 33% of the time, Pallas kernels for 1%

profile of v2, /device:TPU:0, one launch (start us, length us, event | category | flops | bytes accessed | tf_op | source)
XLA Modules:
  0.0 245.0 jit_solution(5296667449338769023)
XLA Ops:
  1.2 3.6 %collective-permute-start.13 = (bf16[256,1024]{1,0:T(8,128)(2,1)}, bf16[256,1024]{1,0:T(8,128)(2,1)S(1)}, u32[]{:S(2)}, u32[]{:S(2)}) collective-permute-start(bf16[256,1024]{1,0:T(8,128)(2,1)} %mine.1), channel_id=1, source_target_pairs={{0,16},{2,18},{4,20},{6,22},{8,24},{10,26},{12,28},{14,30},{16,0},... | collective-permute-start | bytes 1572872 | tf_op jit(solution)/shard_map/ppermute | solution.py:196
  6.3 22.7 %collective-permute-done.7 = f32[4,256]{1,0:T(4,128)S(1)} collective-permute-done((f32[4,256]{1,0:T(4,128)S(1)}, f32[4,256]{1,0:T(4,128)S(1)}, u32[]{:S(2)}, u32[]{:S(2)}) %collective-permute-start.7) | collective-permute-done | bytes 4128 | tf_op jit(solution)/shard_map/ppermute | solution.py:196
  34.7 4.1 %all-to-all-start.1 = ((bf16[8,64,2048]{2,1,0:T(8,128)(2,1)}), bf16[8,64,2048]{2,1,0:T(8,128)(2,1)S(1)}, u32[]{:S(2)}, u32[]{:S(2)}) async-start(bf16[8,64,2048]{2,1,0:T(8,128)(2,1)} %bitcast.10), calls=%async_computation.1 | async-start | bytes 4194304 | tf_op jit(solution)/shard_map/all_to_all | solution.py:24
  38.7 3.4 %collective-permute-start.9 = (bf16[256,1024]{1,0:T(8,128)(2,1)S(1)}, bf16[256,1024]{1,0:T(8,128)(2,1)S(1)}, u32[]{:S(2)}, u32[]{:S(2)}) collective-permute-start(bf16[256,1024]{1,0:T(8,128)(2,1)S(1)} %copy-done.2), channel_id=1, source_target_pairs={{0,16},{2,18},{4,20},{6,22},{8,24},{10,26},{12,28},{14,30},{16,0},... | collective-permute-start | bytes 1572872 | tf_op jit(solution)/shard_map/ppermute | solution.py:196
  42.1 30.9 %collective-permute-done.9 = bf16[256,1024]{1,0:T(8,128)(2,1)S(1)} collective-permute-done((bf16[256,1024]{1,0:T(8,128)(2,1)S(1)}, bf16[256,1024]{1,0:T(8,128)(2,1)S(1)}, u32[]{:S(2)}, u32[]{:S(2)}) %collective-permute-start.9) | collective-permute-done | bytes 524320 | tf_op jit(solution)/shard_map/ppermute | solution.py:196
  81.1 11.7 %all-to-all-start = ((bf16[8,64,2048]{2,1,0:T(8,128)(2,1)}), bf16[8,64,2048]{2,1,0:T(8,128)(2,1)}, u32[]{:S(2)}, u32[]{:S(2)}) async-start(bf16[8,64,2048]{2,1,0:T(8,128)(2,1)} %bitcast.58), calls=%async_computation | async-start | bytes 4194304 | tf_op jit(solution)/shard_map/all_to_all | solution.py:24
  92.8 5.0 %pad_maximum_fusion.1.gate = bf16[4,4,128,1024]{3,2,1,0:T(8,128)(2,1)} fusion(bf16[4,4,128,512]{3,2,1,0:T(8,128)(2,1)} %bitcast.15, bf16[4,4,128,512]{3,2,1,0:T(8,128)(2,1)} %bitcast.65), kind=kLoop, calls=%fused_computation.9 | loop fusion | flops 8388608 | bytes 8388608 | tf_op jit(solution)/shard_map/concatenate | solution.py:273
  97.8 4.4 %pad_maximum_fusion.2.up = bf16[4,4,128,1024]{3,2,1,0:T(8,128)(2,1)} fusion(bf16[4,4,128,512]{3,2,1,0:T(8,128)(2,1)} %bitcast.17, bf16[4,4,128,512]{3,2,1,0:T(8,128)(2,1)S(1)} %bitcast.62), kind=kLoop, calls=%fused_computation.10 | loop fusion | flops 8388608 | bytes 8388608 | tf_op jit(solution)/shard_map/concatenate | solution.py:274
  102.2 4.2 %pad_maximum_fusion.down = bf16[1024,2048]{1,0:T(8,128)(2,1)} fusion(bf16[512,2048]{1,0:T(8,128)(2,1)} %collective-permute-done.11, bf16[512,2048]{1,0:T(8,128)(2,1)S(1)} %bitcast.60), kind=kLoop, calls=%fused_computation | loop fusion | flops 8388608 | bytes 8388608 | tf_op jit(solution)/shard_map/concatenate | solution.py:275
  106.4 4.1 %fusion.4 = f32[512,1024]{1,0:T(8,128)S(1)} fusion(bf16[512,2048]{1,0:T(8,128)(2,1)S(1)} %bitcast.52, bf16[2048,512]{1,0:T(8,128)(2,1)} %collective-permute-done.16, bf16[2048,512]{1,0:T(8,128)(2,1)S(1)} %bitcast.63), kind=kOutput, calls=%fused_computation.5 | convolution fusion | flops 2155872256 | bytes 8388608 | tf_op jit(solution)/shard_map/dot_general | solution.py:38
  110.5 7.0 %add_multiply_fusion = (f32[512,1024]{1,0:T(8,128)}, bf16[512,1024]{1,0:T(8,128)(2,1)}, f32[512,1024]{1,0:T(8,128)}) fusion(f32[512,1024]{1,0:T(8,128)S(1)} %fusion.4, bf16[512,2048]{1,0:T(8,128)(2,1)S(1)} %bitcast.53, bf16[2048,512]{1,0:T(8,128)(2,1)} %collective-permute-done.15, bf16[2048,512]{1,0:T(8,128)(2,1)S(1)} %bitcast.66), kind=kOutput, calls=%fused_computation.26 | convolution fusion | flops 2161639424 | bytes 13631488 | tf_op jit(solution)/shard_map/dot_general | solution.py:38
  118.9 13.6 %row_grads.1 = (bf16[512,1024]{1,0:T(8,128)(2,1)}, bf16[512,1024]{1,0:T(8,128)(2,1)}, bf16[4,4,128,512]{3,2,1,0:T(8,128)(2,1)}) custom-call(bf16[512,2048]{1,0:T(8,128)(2,1)} %bitcast.8.cot, bf16[1024,2048]{1,0:T(8,128)(2,1)} %pad_maximum_fusion.down, f32[512,1024]{1,0:T(8,128)} %get-tuple-element.16.silu, f32[512,1024]{1,0:T(8,128)} %get-tuple-element.17.slope, ...), custom_call_target="tpu_custom_call" | custom-call | flops 6442450944 | bytes 16777216 | tf_op jit(solution)/shard_map/row_grads/pallas_call | solution.py:83
  132.6 5.8 %all-to-all-start.2 = ((bf16[16,128,512]{2,1,0:T(8,128)(2,1)}), bf16[16,128,512]{2,1,0:T(8,128)(2,1)S(1)}, u32[]{:S(2)}, u32[]{:S(2)}) async-start(bf16[16,128,512]{2,1,0:T(8,128)(2,1)} %bitcast.57), calls=%async_computation.2 | async-start | bytes 4194304 | tf_op jit(solution)/shard_map/all_to_all | solution.py:24
  149.8 6.5 %collective-permute-done.5 = f32[2,256]{1,0:T(2,128)} collective-permute-done((f32[2,256]{1,0:T(2,128)S(1)}, f32[2,256]{1,0:T(2,128)}, u32[]{:S(2)}, u32[]{:S(2)}) %collective-permute-start.5) | collective-permute-done | bytes 2080 | tf_op jit(solution)/shard_map/ppermute | solution.py:186
  156.3 4.0 %collective-permute-start.22 = (f32[2,512]{1,0:T(2,128)}, f32[2,512]{1,0:T(2,128)}, u32[]{:S(2)}, u32[]{:S(2)}) collective-permute-start(f32[2,512]{1,0:T(2,128)} %slice.109), channel_id=1, source_target_pairs={{0,2},{2,4},{4,6},{6,8},{8,10},{10,12},{12,14},{14,16},{16,18},{18... | collective-permute-start | bytes 12296 | tf_op jit(solution)/shard_map/ppermute | solution.py:16
  163.4 2.9 %copy.22 = s32[512,1024]{0,1:T(8,128)} copy(s32[512,1024]{1,0:T(8,128)} %bitcast.51) | data formatting | bytes 4194304 | tf_op jit(solution)/shard_map/eq | solution.py:269
  168.7 2.8 %fusion.37.pick = bf16[1024,512]{1,0:T(8,128)(2,1)} fusion(s32[512,1024]{0,1:T(8,128)} %copy.22, s32[512]{0:T(512)S(1)} %copy-done.27), kind=kLoop, calls=%fused_computation.43 | loop fusion | flops 1048576 | bytes 3147776 | tf_op jit(solution)/shard_map/transpose | solution.py:270
  173.5 5.2 %maximum_select_fusion.out_cut = bf16[1024,512]{1,0:T(8,128)(2,1)S(1)} fusion(bf16[1024,256]{1,0:T(8,128)(2,1)S(1)} %collective-permute-done.3, bf16[256,256]{1,0:T(8,128)(2,1)S(1)} %copy-done.19, bf16[256,256]{1,0:T(8,128)(2,1)S(1)} %copy-done.21, bf16[256,256]{1,0:T(8,128)(2,1)S(1)} %copy-done.23, bf16[256,128]{1,0:T(8,128)(2,1)S(1)} %get-tuple-element.53, ...), kind=kLoop, calls=%fused_computation.44 | loop fusion | flops 13107200 | bytes 2097153 | tf_op jit(solution)/shard_map/jit(_where)/select_n | solution.py:30
  184.0 3.5 %collective-permute-start.26 = (bf16[256,512]{1,0:T(8,128)(2,1)S(1)}, bf16[256,512]{1,0:T(8,128)(2,1)S(1)}, u32[]{:S(2)}, u32[]{:S(2)}) collective-permute-start(bf16[256,512]{1,0:T(8,128)(2,1)S(1)} %copy-done.26), channel_id=1, source_target_pairs={{0,6},{2,4},{4,2},{6,0},{8,14},{10,12},{12,10},{14,8},{16,22},{18,... | collective-permute-start | bytes 786440 | tf_op jit(solution)/shard_map/ppermute | solution.py:186
  187.5 6.1 %convolution_bitcast_fusion.1 = f32[1,2048,512]{2,1,0:T(8,128)} fusion(bf16[512,2048]{1,0:T(8,128)(2,1)} %collective-permute-done.30, bf16[512,2048]{1,0:T(8,128)(2,1)S(1)} %bitcast.55, bf16[512,512]{1,0:T(8,128)(2,1)} %collective-permute-done.31, bf16[512,512]{1,0:T(8,128)(2,1)S(1)} %copy-done.17), kind=kOutput, calls=%fused_computation.22 | convolution fusion | flops 2157969408 | bytes 9437184 | tf_op jit(solution)/shard_map/dot_general | solution.py:38
  194.6 6.1 %convolution_bitcast_fusion = f32[1,2048,512]{2,1,0:T(8,128)} fusion(bf16[512,2048]{1,0:T(8,128)(2,1)} %collective-permute-done.30, bf16[512,2048]{1,0:T(8,128)(2,1)S(1)} %bitcast.56, bf16[512,512]{1,0:T(8,128)(2,1)} %collective-permute-done.32, bf16[512,512]{1,0:T(8,128)(2,1)S(1)} %copy-done.16), kind=kOutput, calls=%fused_computation.21 | convolution fusion | flops 2157969408 | bytes 9437184 | tf_op jit(solution)/shard_map/dot_general | solution.py:38
  207.6 12.5 %collective-permute-start.29 = (bf16[128,512]{1,0:T(8,128)(2,1)S(1)}, bf16[128,512]{1,0:T(8,128)(2,1)S(1)}, u32[]{:S(2)}, u32[]{:S(2)}) collective-permute-start(bf16[128,512]{1,0:T(8,128)(2,1)S(1)} %get-tuple-element.38), channel_id=1, source_target_pairs={{0,8},{2,10},{4,12},{6,14},{8,0},{10,2},{12,4},{14,6},{16,24},{18,... | collective-permute-start | bytes 393224 | tf_op jit(solution)/shard_map/ppermute | solution.py:186
  220.1 6.9 %collective-permute-start.28 = (bf16[128,512]{1,0:T(8,128)(2,1)S(1)}, bf16[128,512]{1,0:T(8,128)(2,1)S(1)}, u32[]{:S(2)}, u32[]{:S(2)}) collective-permute-start(bf16[128,512]{1,0:T(8,128)(2,1)S(1)} %get-tuple-element.39), channel_id=1, source_target_pairs={{0,16},{2,18},{4,20},{6,22},{8,24},{10,26},{12,28},{14,30},{16,0},... | collective-permute-start | bytes 393224 | tf_op jit(solution)/shard_map/ppermute | solution.py:186
  228.1 6.8 %fusion.15 = f32[1,512,2048]{2,1,0:T(8,128)} fusion(bf16[512,2048]{1,0:T(8,128)(2,1)} %collective-permute-done.34, bf16[512,2048]{1,0:T(8,128)(2,1)} %bitcast.8.cot, bf16[512,512]{1,0:T(8,128)(2,1)S(1)} %collective-permute-done.33, bf16[512,512]{1,0:T(8,128)(2,1)S(1)} %get-tuple-element.31), kind=kOutput, calls=%fused_computation.20 | convolution fusion | flops 2157969408 | bytes 9437184 | tf_op jit(solution)/shard_map/dot_general | solution.py:38
  (178 shorter events, 60.1 us)
Async XLA Ops:
  0.6 29.9 %collective-permute-start.12 = (bf16[256,1024]{1,0:T(8,128)(2,1)}, bf16[256,1024]{1,0:T(8,128)(2,1)S(1)}, u32[]{:S(2)}, u32[]{:S(2)}) collective-permute-start(bf16[256,1024]{1,0:T(8,128)(2,1)} %mine.1), channel_id=1, source_target_pairs={{0,1},{1,0},{2,3},{3,2},{4,5},{5,4},{6,7},{7,6},{8,9},{9,8},{10,11... | collective-permute-start | bytes 1572872 | tf_op jit(solution)/shard_map/ppermute | solution.py:20
  1.2 28.9 %collective-permute-start.13 = (bf16[256,1024]{1,0:T(8,128)(2,1)}, bf16[256,1024]{1,0:T(8,128)(2,1)S(1)}, u32[]{:S(2)}, u32[]{:S(2)}) collective-permute-start(bf16[256,1024]{1,0:T(8,128)(2,1)} %mine.1), channel_id=1, source_target_pairs={{0,16},{2,18},{4,20},{6,22},{8,24},{10,26},{12,28},{14,30},{16,0},... | collective-permute-start | bytes 1572872 | tf_op jit(solution)/shard_map/ppermute | solution.py:196
  6.2 22.8 %collective-permute-start.7 = (f32[4,256]{1,0:T(4,128)S(1)}, f32[4,256]{1,0:T(4,128)S(1)}, u32[]{:S(2)}, u32[]{:S(2)}) collective-permute-start(f32[4,256]{1,0:T(4,128)S(1)} %pad_maximum_fusion.13), channel_id=1, source_target_pairs={{0,16},{2,18},{4,20},{6,22},{8,24},{10,26},{12,28},{14,30},{16,0},... | collective-permute-start | bytes 12296 | tf_op jit(solution)/shard_map/ppermute | solution.py:196
  34.7 46.5 %all-to-all-start.1 = ((bf16[8,64,2048]{2,1,0:T(8,128)(2,1)}), bf16[8,64,2048]{2,1,0:T(8,128)(2,1)S(1)}, u32[]{:S(2)}, u32[]{:S(2)}) async-start(bf16[8,64,2048]{2,1,0:T(8,128)(2,1)} %bitcast.10), calls=%async_computation.1 | async-start | bytes 4194304 | tf_op jit(solution)/shard_map/all_to_all | solution.py:24
  38.7 34.3 %collective-permute-start.9 = (bf16[256,1024]{1,0:T(8,128)(2,1)S(1)}, bf16[256,1024]{1,0:T(8,128)(2,1)S(1)}, u32[]{:S(2)}, u32[]{:S(2)}) collective-permute-start(bf16[256,1024]{1,0:T(8,128)(2,1)S(1)} %copy-done.2), channel_id=1, source_target_pairs={{0,16},{2,18},{4,20},{6,22},{8,24},{10,26},{12,28},{14,30},{16,0},... | collective-permute-start | bytes 1572872 | tf_op jit(solution)/shard_map/ppermute | solution.py:196
  42.1 33.0 %collective-permute-start.8 = (bf16[256,1024]{1,0:T(8,128)(2,1)S(1)}, bf16[256,1024]{1,0:T(8,128)(2,1)}, u32[]{:S(2)}, u32[]{:S(2)}) collective-permute-start(bf16[256,1024]{1,0:T(8,128)(2,1)S(1)} %copy-done.2), channel_id=1, source_target_pairs={{0,1},{1,0},{2,3},{3,2},{4,5},{5,4},{6,7},{7,6},{8,9},{9,8},{10,11... | collective-permute-start | bytes 1572872 | tf_op jit(solution)/shard_map/ppermute | solution.py:20
  73.0 29.1 %collective-permute-start.11 = (bf16[512,2048]{1,0:T(8,128)(2,1)}, bf16[512,2048]{1,0:T(8,128)(2,1)}, u32[]{:S(2)}, u32[]{:S(2)}) collective-permute-start(bf16[512,2048]{1,0:T(8,128)(2,1)} %bitcast.59), channel_id=1, source_target_pairs={{0,1},{1,0},{2,3},{3,2},{4,5},{5,4},{6,7},{7,6},{8,9},{9,8},{10,11... | collective-permute-start | bytes 6291464 | tf_op jit(solution)/shard_map/ppermute | solution.py:20
  73.5 24.3 %collective-permute-start.16 = (bf16[2048,512]{1,0:T(8,128)(2,1)}, bf16[2048,512]{1,0:T(8,128)(2,1)}, u32[]{:S(2)}, u32[]{:S(2)}) collective-permute-start(bf16[2048,512]{1,0:T(8,128)(2,1)} %bitcast.61), channel_id=1, source_target_pairs={{0,1},{1,0},{2,3},{3,2},{4,5},{5,4},{6,7},{7,6},{8,9},{9,8},{10,11... | collective-permute-start | bytes 6291464 | tf_op jit(solution)/shard_map/ppermute | solution.py:20
  73.5 19.3 %collective-permute-start.15 = (bf16[2048,512]{1,0:T(8,128)(2,1)}, bf16[2048,512]{1,0:T(8,128)(2,1)}, u32[]{:S(2)}, u32[]{:S(2)}) collective-permute-start(bf16[2048,512]{1,0:T(8,128)(2,1)} %bitcast.64), channel_id=1, source_target_pairs={{0,1},{1,0},{2,3},{3,2},{4,5},{5,4},{6,7},{7,6},{8,9},{9,8},{10,11... | collective-permute-start | bytes 6291464 | tf_op jit(solution)/shard_map/ppermute | solution.py:20
  81.1 37.8 %all-to-all-start = ((bf16[8,64,2048]{2,1,0:T(8,128)(2,1)}), bf16[8,64,2048]{2,1,0:T(8,128)(2,1)}, u32[]{:S(2)}, u32[]{:S(2)}) async-start(bf16[8,64,2048]{2,1,0:T(8,128)(2,1)} %bitcast.58), calls=%async_computation | async-start | bytes 4194304 | tf_op jit(solution)/shard_map/all_to_all | solution.py:24
  132.6 48.9 %all-to-all-start.2 = ((bf16[16,128,512]{2,1,0:T(8,128)(2,1)}), bf16[16,128,512]{2,1,0:T(8,128)(2,1)S(1)}, u32[]{:S(2)}, u32[]{:S(2)}) async-start(bf16[16,128,512]{2,1,0:T(8,128)(2,1)} %bitcast.57), calls=%async_computation.2 | async-start | bytes 4194304 | tf_op jit(solution)/shard_map/all_to_all | solution.py:24
  141.8 18.5 %collective-permute-start.4 = (f32[2,256]{1,0:T(2,128)S(1)}, f32[2,256]{1,0:T(2,128)}, u32[]{:S(2)}, u32[]{:S(2)}) collective-permute-start(f32[2,256]{1,0:T(2,128)S(1)} %convert_bitcast_fusion), channel_id=1, source_target_pairs={{0,2},{2,0},{4,6},{6,4},{8,10},{10,8},{12,14},{14,12},{16,18},{18,... | collective-permute-start | bytes 6152 | tf_op jit(solution)/shard_map/ppermute | solution.py:186
  142.8 23.5 %collective-permute-start.2 = (bf16[256,256]{1,0:T(8,128)(2,1)}, bf16[256,256]{1,0:T(8,128)(2,1)S(1)}, u32[]{:S(2)}, u32[]{:S(2)}) collective-permute-start(bf16[256,256]{1,0:T(8,128)(2,1)} %pad_maximum_fusion.11), channel_id=1, source_target_pairs={{0,6},{2,4},{4,2},{6,0},{8,14},{10,12},{12,10},{14,8},{16,22},{18,... | collective-permute-start | bytes 393224 | tf_op jit(solution)/shard_map/ppermute | solution.py:186
  146.2 20.1 %collective-permute-start.1 = (bf16[256,256]{1,0:T(8,128)(2,1)}, bf16[256,256]{1,0:T(8,128)(2,1)S(1)}, u32[]{:S(2)}, u32[]{:S(2)}) collective-permute-start(bf16[256,256]{1,0:T(8,128)(2,1)} %pad_maximum_fusion.10), channel_id=1, source_target_pairs={{0,4},{2,6},{4,0},{6,2},{8,12},{10,14},{12,8},{14,10},{16,20},{18,... | collective-permute-start | bytes 393224 | tf_op jit(solution)/shard_map/ppermute | solution.py:186
  149.7 16.6 %collective-permute-start = (bf16[256,256]{1,0:T(8,128)(2,1)}, bf16[256,256]{1,0:T(8,128)(2,1)S(1)}, u32[]{:S(2)}, u32[]{:S(2)}) collective-permute-start(bf16[256,256]{1,0:T(8,128)(2,1)} %pad_maximum_fusion.9), channel_id=1, source_target_pairs={{0,2},{2,0},{4,6},{6,4},{8,10},{10,8},{12,14},{14,12},{16,18},{18,... | collective-permute-start | bytes 393224 | tf_op jit(solution)/shard_map/ppermute | solution.py:186
  161.0 26.5 %collective-permute-start.30 = (bf16[512,2048]{1,0:T(8,128)(2,1)}, bf16[512,2048]{1,0:T(8,128)(2,1)}, u32[]{:S(2)}, u32[]{:S(2)}) collective-permute-start(bf16[512,2048]{1,0:T(8,128)(2,1)} %bitcast.54), channel_id=1, source_target_pairs={{0,1},{1,0},{2,3},{3,2},{4,5},{5,4},{6,7},{7,6},{8,9},{9,8},{10,11... | collective-permute-start | bytes 6291464 | tf_op jit(solution)/shard_map/ppermute | solution.py:20
  178.7 49.3 %collective-permute-start.34 = (bf16[512,2048]{1,0:T(8,128)(2,1)}, bf16[512,2048]{1,0:T(8,128)(2,1)}, u32[]{:S(2)}, u32[]{:S(2)}) collective-permute-start(bf16[512,2048]{1,0:T(8,128)(2,1)} %bitcast.8.cot), channel_id=1, source_target_pairs={{0,1},{1,0},{2,3},{3,2},{4,5},{5,4},{6,7},{7,6},{8,9},{9,8},{10,11... | collective-permute-start | bytes 6291464 | tf_op jit(solution)/shard_map/ppermute | solution.py:20
  183.4 17.3 %collective-permute-start.17 = (bf16[1024,512]{1,0:T(8,128)(2,1)S(1)}, bf16[1024,512]{1,0:T(8,128)(2,1)S(1)}, u32[]{:S(2)}, u32[]{:S(2)}) collective-permute-start(bf16[1024,512]{1,0:T(8,128)(2,1)S(1)} %shard_map.180.mine), channel_id=1, source_target_pairs={{0,1},{1,0},{2,3},{3,2},{4,5},{5,4},{6,7},{7,6},{8,9},{9,8},{10,11... | collective-permute-start | bytes 3145736 | tf_op jit(solution)/shard_map/ppermute | solution.py:20
  184.0 17.2 %collective-permute-start.26 = (bf16[256,512]{1,0:T(8,128)(2,1)S(1)}, bf16[256,512]{1,0:T(8,128)(2,1)S(1)}, u32[]{:S(2)}, u32[]{:S(2)}) collective-permute-start(bf16[256,512]{1,0:T(8,128)(2,1)S(1)} %copy-done.26), channel_id=1, source_target_pairs={{0,6},{2,4},{4,2},{6,0},{8,14},{10,12},{12,10},{14,8},{16,22},{18,... | collective-permute-start | bytes 786440 | tf_op jit(solution)/shard_map/ppermute | solution.py:186
  200.7 27.3 %collective-permute-start.33 = (bf16[512,512]{1,0:T(8,128)(2,1)S(1)}, bf16[512,512]{1,0:T(8,128)(2,1)S(1)}, u32[]{:S(2)}, u32[]{:S(2)}) collective-permute-start(bf16[512,512]{1,0:T(8,128)(2,1)S(1)} %get-tuple-element.32), channel_id=1, source_target_pairs={{0,1},{1,0},{2,3},{3,2},{4,5},{5,4},{6,7},{7,6},{8,9},{9,8},{10,11... | collective-permute-start | bytes 1572872 | tf_op jit(solution)/shard_map/ppermute | solution.py:20
  202.3 17.8 %collective-permute-start.19 = (bf16[256,256]{1,0:T(8,128)(2,1)S(1)}, bf16[256,256]{1,0:T(8,128)(2,1)S(1)}, u32[]{:S(2)}, u32[]{:S(2)}) collective-permute-start(bf16[256,256]{1,0:T(8,128)(2,1)S(1)} %get-tuple-element.43), channel_id=1, source_target_pairs={{0,4},{2,6},{4,0},{6,2},{8,12},{10,14},{12,8},{14,10},{16,20},{18,... | collective-permute-start | bytes 393224 | tf_op jit(solution)/shard_map/ppermute | solution.py:186
  204.3 22.7 %collective-permute-start.20 = (bf16[256,256]{1,0:T(8,128)(2,1)S(1)}, bf16[256,256]{1,0:T(8,128)(2,1)S(1)}, u32[]{:S(2)}, u32[]{:S(2)}) collective-permute-start(bf16[256,256]{1,0:T(8,128)(2,1)S(1)} %get-tuple-element.42), channel_id=1, source_target_pairs={{0,6},{2,4},{4,2},{6,0},{8,14},{10,12},{12,10},{14,8},{16,22},{18,... | collective-permute-start | bytes 393224 | tf_op jit(solution)/shard_map/ppermute | solution.py:186
  207.6 27.2 %collective-permute-start.29 = (bf16[128,512]{1,0:T(8,128)(2,1)S(1)}, bf16[128,512]{1,0:T(8,128)(2,1)S(1)}, u32[]{:S(2)}, u32[]{:S(2)}) collective-permute-start(bf16[128,512]{1,0:T(8,128)(2,1)S(1)} %get-tuple-element.38), channel_id=1, source_target_pairs={{0,8},{2,10},{4,12},{6,14},{8,0},{10,2},{12,4},{14,6},{16,24},{18,... | collective-permute-start | bytes 393224 | tf_op jit(solution)/shard_map/ppermute | solution.py:186
  220.1 16.0 %collective-permute-start.28 = (bf16[128,512]{1,0:T(8,128)(2,1)S(1)}, bf16[128,512]{1,0:T(8,128)(2,1)S(1)}, u32[]{:S(2)}, u32[]{:S(2)}) collective-permute-start(bf16[128,512]{1,0:T(8,128)(2,1)S(1)} %get-tuple-element.39), channel_id=1, source_target_pairs={{0,16},{2,18},{4,20},{6,22},{8,24},{10,26},{12,28},{14,30},{16,0},... | collective-permute-start | bytes 393224 | tf_op jit(solution)/shard_map/ppermute | solution.py:186
  (45 other events, 347.2 us)
